TPU v7x, 512 devices: a whole 4x4x16 slice. The times are simulated.
512 devices in a mesh: sp: 32 (over z, core), tp: 16 (over y, x).
Axes of the slice: x: 4, y: 4, z: 16, core: 2. Of those that a mesh axis runs over, the one named last changes fastest.
Arguments:
- residual_in: bfloat16 [8192, 2048], P('sp'), may hold values from -3 to 3
- mix_gain: float32 [2048], replicated, may hold values from 0.1 to 1.9
- pool_weight: bfloat16 [512, 2048], P(None, 'tp'), may hold values from -0.5 to 0.5
- pool_scale: float32 [2048], P('tp'), may hold values from 0.1 to 1.9
- ffn_gain: float32 [2048], replicated, may hold values from 0.1 to 1.9
- route_ids: int32 [8192, 2], P('sp'), may hold values from 0 to 31, all different within a row; in each aligned block of 16 rows (0 to 15, 16 to 31, ...) at most 2 rows name the same one
- route_weights: float32 [8192, 2], P('sp'), may hold values from 0.1 to 1
- gate_weight: bfloat16 [32, 2048, 3584], P('sp', None, 'tp'), may hold values from -0.125 to 0.125
- up_weight: bfloat16 [32, 2048, 3584], P('sp', None, 'tp'), may hold values from -0.125 to 0.125
- down_weight: bfloat16 [32, 3584, 2048], P('sp', 'tp'), may hold values from -0.09375 to 0.09375
Outputs:
- layer_out: bfloat16 [8192, 2048], P('sp')
Inputs may be any that keep to these rules, and one draw needn't show every extreme that they name: `route_ids`: each row names 2 different experts; in each aligned block of 16 rows no expert is named by more than 2 rows, and some block has an expert named by exactly 2 rows.
All inputs are finite; a program needn't handle non-finite values.
Results may differ from a plain program's by a relative error of at most 0.0074.
Values may be sent and summed in bfloat16 or wider, within the bound.
A program may use at most 64 MiB of HBM per device.

v0:
```python
import jax
import jax.numpy as jnp
from jax import lax
from jax.sharding import Mesh
from jax.sharding import PartitionSpec as P

GROUPS = 4
SPAN = 16
TOP_K = 2
SP = ("sp_0", "sp_1")


EPS = 1e-06


def from_behind(value, axis, steps):
    count = lax.axis_size(axis)
    first, last = (max(0, -steps), min(count, count - steps))
    return lax.ppermute(value, axis, [(source, source + steps) for source in range(first, last)])


def split_up(shard, dim, size):
    before, after = (shard.shape[:dim], shard.shape[dim + 1 :])
    return jnp.moveaxis(shard.reshape(*before, size, -1, *after), dim, 0)


def sent_and_summed(shard, axis, dim):
    size = lax.axis_size(axis)
    blocks = lax.all_to_all(split_up(shard, dim, size), axis, 0, 0, tiled=True)
    return jnp.sum(blocks.astype(jnp.float32), axis=0)


def in_order(blocks, dim):
    dims = list(blocks.shape[1:])
    dims[dim] *= blocks.shape[0]
    return jnp.moveaxis(blocks, 0, dim).reshape(dims)


def exchange_in_order(blocks, axes, order):
    dims = [lax.axis_size(a) for a in axes]
    blocks = blocks.reshape(*dims, *blocks.shape[1:])
    for k in order:
        blocks = lax.all_to_all(blocks, axes[k], split_axis=k, concat_axis=k, tiled=True)
    return blocks.reshape(-1, *blocks.shape[len(axes) :])


def core_and_chips(shard, groups, order, split_dim, concat_dim):
    size = lax.axis_size(groups[0]) * lax.axis_size(groups[1])
    blocks = split_up(shard, split_dim, size)
    return in_order(exchange_in_order(blocks, groups, order), concat_dim)


def copy_for_each(shard, axis):
    size = lax.axis_size(axis)
    return lax.all_to_all(
        jnp.broadcast_to(shard[None], (size, *shard.shape)), axis, 0, 0, tiled=True
    )


def gather_directly(shard, axis, dim):
    blocks = copy_for_each(shard, axis)
    return in_order(blocks, dim)


def rms_scale(values, gain):
    return values * lax.rsqrt(jnp.mean(values * values, axis=-1, keepdims=True) + EPS) * gain


def slot_table(chosen_ids, experts, capacity):
    flat_ids = chosen_ids.reshape(-1)
    matches = (flat_ids[:, None] == jnp.arange(experts, dtype=jnp.int32)[None, :]).astype(jnp.int32)
    before = jnp.cumsum(matches, axis=0) - matches
    slot_of = jnp.sum(before * matches, axis=1)
    target = flat_ids * capacity + slot_of
    return (target[:, None] == jnp.arange(experts * capacity, dtype=jnp.int32)[None, :]).astype(
        jnp.float32
    )


def shards(
    residual_in,
    mix_gain,
    pool_weight,
    pool_scale,
    ffn_gain,
    route_ids,
    route_weights,
    gate_weight,
    up_weight,
    down_weight,
):
    tp_count = lax.axis_size("tp")
    sp_count = lax.axis_size(SP)
    tp_index = lax.axis_index("tp")
    tok_count, width = residual_in.shape
    group_width = width // GROUPS
    col_count = pool_weight.shape[1]
    row_count = tok_count // tp_count
    capacity = 2 * TOP_K * row_count // sp_count
    group_index = tp_index * col_count // group_width
    window = jnp.power(2, group_index + 1)
    stream = residual_in.astype(jnp.float32)
    inverse = lax.rsqrt(jnp.mean(stream * stream, axis=-1, keepdims=True) + EPS)
    stream_group = lax.dynamic_slice_in_dim(stream, group_index * group_width, group_width, 1)
    gain_group = lax.dynamic_slice_in_dim(mix_gain, group_index * group_width, group_width, 0)
    normed_group = (stream_group * inverse * gain_group).astype(jnp.bfloat16)
    rim_rows = from_behind(normed_group[tok_count - SPAN :], SP, 1)
    extended = jnp.concatenate([rim_rows, normed_group], axis=0).astype(jnp.float32)
    window_sum = jnp.zeros((tok_count, group_width), jnp.float32)
    for offset in range(SPAN):
        window_sum = window_sum + jnp.where(
            offset < window, extended[SPAN - offset : SPAN - offset + tok_count], 0.0
        )
    position = lax.axis_index(SP) * tok_count + jnp.arange(tok_count, dtype=jnp.int32)
    divisor = jnp.minimum(position + 1, window).astype(jnp.float32)
    pooled = (window_sum / divisor[:, None] - extended[SPAN:]).astype(jnp.bfloat16)
    mixed = (jnp.dot(pooled, pool_weight, preferred_element_type=jnp.float32) * pool_scale).astype(
        jnp.bfloat16
    )
    stream_own = lax.dynamic_slice_in_dim(stream, tp_index * row_count, row_count, 0)
    mixed_own = lax.all_to_all(mixed, "tp", split_axis=0, concat_axis=1, tiled=True)
    after_own = (stream_own + mixed_own.astype(jnp.float32)).astype(jnp.bfloat16)
    normed_own = rms_scale(after_own.astype(jnp.float32), ffn_gain).astype(jnp.bfloat16)
    ids_own = lax.dynamic_slice_in_dim(route_ids, tp_index * row_count, row_count, 0)
    table_own = slot_table(ids_own, sp_count, capacity)
    repeated = jnp.repeat(normed_own, TOP_K, axis=0)
    outgoing = lax.dot_general(
        table_own.astype(jnp.bfloat16),
        repeated,
        (((0,), (0,)), ((), ())),
        preferred_element_type=jnp.float32,
    )
    outgoing = outgoing.astype(jnp.bfloat16).reshape(sp_count, capacity, width)
    arrived = lax.all_to_all(outgoing, SP, split_axis=0, concat_axis=0, tiled=True)
    piece = lax.all_gather(arrived, "tp", axis=0, tiled=True)
    flat_rows = piece.reshape(-1, width)
    gate_part = jnp.dot(flat_rows, gate_weight[0], preferred_element_type=jnp.float32)
    up_part = jnp.dot(flat_rows, up_weight[0], preferred_element_type=jnp.float32)
    hidden = (jax.nn.silu(gate_part) * up_part).astype(jnp.bfloat16)
    hidden_all = hidden.reshape(piece.shape[0], piece.shape[1], hidden.shape[1])
    hidden_flat = hidden_all.reshape(-1, hidden_all.shape[-1])
    term = jnp.dot(hidden_flat, down_weight[0], preferred_element_type=jnp.float32)
    summed = sent_and_summed(
        term.astype(jnp.bfloat16).astype(jnp.float32).astype(jnp.bfloat16), "tp", 0
    )
    expert_out = summed.astype(jnp.bfloat16).reshape(sp_count, capacity, width)
    returned_rows = core_and_chips(expert_out, ("sp_0", "sp_1"), (1, 0), 0, 0)
    weights_own = lax.dynamic_slice_in_dim(route_weights, tp_index * row_count, row_count, 0)
    weight_table = jnp.einsum(
        "rk,rkc->rc", weights_own, table_own.reshape(row_count, TOP_K, sp_count * capacity)
    )
    expert_mix = jnp.dot(
        weight_table,
        returned_rows.reshape(-1, width).astype(jnp.float32),
        precision=lax.Precision.HIGHEST,
    )
    out_own = (after_own.astype(jnp.float32) + expert_mix).astype(jnp.bfloat16)
    return gather_directly(out_own, "tp", 0)


def solution(mesh):
    torus = Mesh(mesh.devices.reshape(16, 2, mesh.shape["tp"]), ("sp_0", "sp_1", "tp"))
    return jax.shard_map(
        shards,
        mesh=torus,
        in_specs=(
            P(SP, None),
            P(),
            P(None, "tp"),
            P("tp"),
            P(),
            P(SP, None),
            P(SP, None),
            P(SP, None, "tp"),
            P(SP, None, "tp"),
            P(SP, "tp", None),
        ),
        out_specs=P(SP, None),
        check_vma=False,
    )
```

profile of v0, /device:TPU:32, one launch (start us, length us, event | category | flops | bytes accessed | tf_op | source)
XLA Modules:
  0.0 268.7 jit_solution(1426922073096499499)
XLA Ops:
  6.5 1.6 multiply_reduce_fusion
  8.1 1.5 convert_element_type.67
  9.6 0.8 dynamic_slice.17
  10.4 0.1 multiply_convert_fusion
  10.5 1.9 collective-permute-start
  12.5 0.1 constant_dynamic-slice_fusion
  12.6 0.1 copy.24
  12.7 0.1 eq.35
  12.8 0.1 fusion.40
  12.8 0.1 reduce_window_sum.11
  12.9 0.2 select_reduce_fusion
  13.1 2.5 collective-permute-done
  15.6 0.1 maximum_convert_fusion
  15.7 0.0 copy-start.1
  15.7 2.0 fusion.2
  17.7 7.0 %all-to-all-start = ((bf16[16,16,128]{2,1,0:T(8,128)(2,1)}), bf16[16,16,128]{2,1,0:T(8,128)(2,1)S(1)}, u32[]{:S(2)}, u32[]{:S(2)}) async-start(bf16[16,16,128]{2,1,0:T(8,128)(2,1)} %bitcast), calls=%async_computation | async-start | bytes 131072 | tf_op jit(solution)/shard_map/all_to_all | solution.py:121
  24.8 0.0 all-gather.2.cloned.1.call-start
  24.8 7.6 %all-to-all-done = bf16[16,16,128]{2,1,0:T(8,128)(2,1)S(1)} async-done(((bf16[16,16,128]{2,1,0:T(8,128)(2,1)}), bf16[16,16,128]{2,1,0:T(8,128)(2,1)S(1)}, u32[]{:S(2)}, u32[]{:S(2)}) %all-to-all-start) | async-done | bytes 65568 | tf_op jit(solution)/shard_map/all_to_all | solution.py:121
  32.4 0.1 fusion.33
  32.6 0.1 fusion.35
  32.7 0.1 broadcast_in_dim.38
  32.8 0.1 reshape.67
  32.8 0.3 convolution_convert_fusion.1
  33.2 0.2 reshape.68
  33.3 37.4 %all_to_all.38 = bf16[32,2,2048]{2,1,0:T(2,128)(2,1)} all-to-all(bf16[32,2,2048]{2,1,0:T(2,128)(2,1)S(1)} %reshape.68), channel_id=1, replica_groups=mesh['sp_0'=16,'sp_1'=2,'tp'=16] {'sp_0','sp_1'}, dimensions={0} | all-to-all | bytes 524288 | tf_op jit(solution)/shard_map/all_to_all | solution.py:134
  70.8 0.0 all-gather.2.cloned.1.call-update
  70.8 0.0 copy-start.3
  70.8 56.0 %all-gather.2.cloned.1.call-done = bf16[512,2,2048]{2,1,0:T(2,128)(2,1)} async-done(((bf16[32,2,2048]{2,1,0:T(2,128)(2,1)}), bf16[512,2,2048]{2,1,0:T(2,128)(2,1)}) %all-gather.2.cloned.1.call-update) | async-done | bytes 4194320 | tf_op jit(solution)/shard_map/all_gather | solution.py:135
  126.8 7.2 %reshape.69 = bf16[1024,2048]{1,0:T(8,128)(2,1)} reshape(bf16[512,2,2048]{2,1,0:T(2,128)(2,1)} %all-gather.2.cloned.1.call-done) | data formatting | bytes 8388608 | tf_op jit(solution)/shard_map/reshape | solution.py:136
  134.0 4.6 %fusion.6 = f32[1024,224]{0,1:T(8,128)} fusion(bf16[1024,2048]{1,0:T(8,128)(2,1)} %reshape.69, bf16[1,2048,224]{1,2,0:T(8,128)(2,1)S(1)} %copy-done.3), kind=kOutput, calls=%fused_computation.11 | convolution fusion | flops 939524096 | bytes 6029312 | tf_op jit(solution)/shard_map/dot_general | solution.py:137
  138.6 7.0 %convolution_convert_fusion = bf16[1024,2048]{1,0:T(8,128)(2,1)} fusion(bf16[1024,2048]{1,0:T(8,128)(2,1)} %reshape.69, bf16[1,224,2048]{2,1,0:T(8,128)(2,1)S(1)} %copy-done, bf16[1,2048,224]{1,2,0:T(8,128)(2,1)S(1)} %copy-done.4, f32[1024,224]{0,1:T(8,128)} %fusion.6), kind=kOutput, calls=%fused_computation | convolution fusion | flops 1882521600 | bytes 11141120 | tf_op jit(solution)/shard_map/dot_general | solution.py:142
  145.6 56.0 %all_to_all.39 = bf16[16,64,2048]{2,1,0:T(8,128)(2,1)} all-to-all(bf16[16,64,2048]{2,1,0:T(8,128)(2,1)} %bitcast.35), channel_id=1, replica_groups=mesh['sp_0'=16,'sp_1'=2,'tp'=16] {'tp'}, dimensions={0} | all-to-all | bytes 8388608 | tf_op jit(solution)/shard_map/all_to_all | solution.py:29
  201.7 3.0 %reduce_sum.45 = bf16[64,2048]{1,0:T(8,128)(2,1)S(1)} reduce(bf16[16,64,2048]{2,1,0:T(8,128)(2,1)} %all_to_all.39, bf16[]{:T(256)} %constant.97.clone.1), dimensions={0}, to_apply=%region_4.5 | reduce | flops 1966080 | bytes 4456450 | tf_op jit(solution)/shard_map/reduce_sum | solution.py:30
  204.6 0.2 reshape_reshape_reshape.6
  204.8 0.2 copy.20
  205.0 3.9 %all_to_all.40 = bf16[16,2,1,2,2048]{4,3,0,2,1:T(2,128)(2,1)S(1)} all-to-all(bf16[16,2,1,2,2048]{4,3,0,2,1:T(2,128)(2,1)S(1)} %copy.20), channel_id=1, replica_groups=mesh['sp_0'=16,'sp_1'=2,'tp'=16] {'sp_1'}, dimensions={1} | all-to-all | bytes 524288 | tf_op jit(solution)/shard_map/all_to_all | solution.py:43
  209.0 1.0 copy.21
  209.9 12.7 %all-to-all-start.4 = ((bf16[16,2,1,2,2048]{4,3,1,2,0:T(2,128)(2,1)}), bf16[16,2,1,2,2048]{4,3,1,2,0:T(2,128)(2,1)S(1)}, u32[]{:S(2)}, u32[]{:S(2)}) async-start(bf16[16,2,1,2,2048]{4,3,1,2,0:T(2,128)(2,1)} %copy.21), calls=%async_computation.4 | async-start | bytes 524288 | tf_op jit(solution)/shard_map/all_to_all | solution.py:43
  222.6 0.1 reduce_sum.43
  222.7 0.8 dynamic-slice_bitcast_fusion
  223.4 0.1 copy.22
  223.5 0.2 fusion.37
  223.7 17.2 %all-to-all-done.4 = bf16[16,2,1,2,2048]{4,3,1,2,0:T(2,128)(2,1)S(1)} async-done(((bf16[16,2,1,2,2048]{4,3,1,2,0:T(2,128)(2,1)}), bf16[16,2,1,2,2048]{4,3,1,2,0:T(2,128)(2,1)S(1)}, u32[]{:S(2)}, u32[]{:S(2)}) %all-to-all-start.4) | async-done | bytes 262176 | tf_op jit(solution)/shard_map/all_to_all | solution.py:43
  241.0 0.1 reshape_reshape_reshape.7
  241.1 0.2 fusion
  241.3 0.1 broadcast_in_dim.39
  241.4 19.5 %all_to_all.41 = bf16[16,16,2048]{2,1,0:T(8,128)(2,1)S(1)} all-to-all(bf16[16,16,2048]{2,1,0:T(8,128)(2,1)S(1)} %broadcast_in_dim.39), channel_id=1, replica_groups=mesh['sp_0'=16,'sp_1'=2,'tp'=16] {'tp'}, dimensions={0} | all-to-all | bytes 2097152 | tf_op jit(solution)/shard_map/all_to_all | solution.py:55
  260.9 1.0 copy.29
  (18 shorter events, 0.1 us)
Async XLA Ops:
  6.5 132.1 %copy-start = (bf16[1,224,2048]{2,1,0:T(8,128)(2,1)S(1)}, bf16[1,224,2048]{2,1,0:T(8,128)(2,1)}, u32[]{:S(2)}) copy-start(bf16[1,224,2048]{2,1,0:T(8,128)(2,1)} %param.19) | copy-start | bytes 2752516
  6.5 6.0 %copy-start.2 = (s32[256,2]{0,1:T(2,128)S(1)}, s32[256,2]{0,1:T(2,128)}, u32[]{:S(2)}) copy-start(s32[256,2]{0,1:T(2,128)} %param.15) | copy-start | bytes 6148
  6.5 9.1 %copy-start.6 = (f32[128]{0:T(128)S(1)}, f32[128]{0:T(128)}, u32[]{:S(2)}) copy-start(f32[128]{0:T(128)} %param.13) | copy-start | bytes 1540
  6.5 9.1 %copy-start.5 = (bf16[512,128]{1,0:T(8,128)(2,1)S(1)}, bf16[512,128]{1,0:T(8,128)(2,1)}, u32[]{:S(2)}) copy-start(bf16[512,128]{1,0:T(8,128)(2,1)} %param.12) | copy-start | bytes 393220
  10.5 5.1 %collective-permute-start = (bf16[16,512]{1,0:T(8,128)(2,1)S(1)}, bf16[16,512]{1,0:T(8,128)(2,1)S(1)}, u32[]{:S(2)}, u32[]{:S(2)}) collective-permute-start(bf16[16,512]{1,0:T(8,128)(2,1)S(1)} %slice.69), channel_id=1, source_target_pairs={{0,16},{16,32},{32,48},{48,64},{64,80},{80,96},{96,112},{112,128},... | collective-permute-start | bytes 49160 | tf_op jit(solution)/shard_map/ppermute | solution.py:19
  15.7 16.9 %copy-start.1 = (f32[2048]{0:T(1024)S(1)}, f32[2048]{0:T(1024)}, u32[]{:S(2)}) copy-start(f32[2048]{0:T(1024)} %param.14) | copy-start | bytes 24580
  17.7 14.7 %all-to-all-start = ((bf16[16,16,128]{2,1,0:T(8,128)(2,1)}), bf16[16,16,128]{2,1,0:T(8,128)(2,1)S(1)}, u32[]{:S(2)}, u32[]{:S(2)}) async-start(bf16[16,16,128]{2,1,0:T(8,128)(2,1)} %bitcast), calls=%async_computation | async-start | bytes 131072 | tf_op jit(solution)/shard_map/all_to_all | solution.py:121
  24.8 102.0 %all-gather.2.cloned.1.call-start = ((), (), s32[]{:S(2)}) async-start(), calls=%async_computation.6 | async-start | bytes 4456448 | tf_op jit(solution)/shard_map/all_gather | solution.py:135
  70.8 63.2 %copy-start.3 = (bf16[1,2048,224]{1,2,0:T(8,128)(2,1)S(1)}, bf16[1,2048,224]{1,2,0:T(8,128)(2,1)}, u32[]{:S(2)}) copy-start(bf16[1,2048,224]{1,2,0:T(8,128)(2,1)} %param.17) | copy-start | bytes 2752516
  134.0 4.6 %copy-start.4 = (bf16[1,2048,224]{1,2,0:T(8,128)(2,1)S(1)}, bf16[1,2048,224]{1,2,0:T(8,128)(2,1)}, u32[]{:S(2)}) copy-start(bf16[1,2048,224]{1,2,0:T(8,128)(2,1)} %param.18) | copy-start | bytes 2752516
  209.9 31.0 %all-to-all-start.4 = ((bf16[16,2,1,2,2048]{4,3,1,2,0:T(2,128)(2,1)}), bf16[16,2,1,2,2048]{4,3,1,2,0:T(2,128)(2,1)S(1)}, u32[]{:S(2)}, u32[]{:S(2)}) async-start(bf16[16,2,1,2,2048]{4,3,1,2,0:T(2,128)(2,1)} %copy.21), calls=%async_computation.4 | async-start | bytes 524288 | tf_op jit(solution)/shard_map/all_to_all | solution.py:43
Sparse Core Ops, SparseCore 0:
  70.9 55.8 all-gather.1
where the time goes:
time: 269 us
  blocking collectives  117 us (43%)
  waiting for transfers between devices  83.3 us (31%)
  starting transfers between devices  21.7 us (8%)
  matrix products  14.4 us (5%)
  between operations  13.7 us (5%)
  local copies, waits for them, and re-layouts  12 us (4%)
  other arithmetic  6.75 us (3%)
    all_to_all x1, blocking collectives, sent_and_summed(): blocks = lax.all_to_all(split_up(shard, dim, size), axis, 0, 0, tiled=True)  56 us
    all_gather x1, waiting for transfers between devices, shards(): piece = lax.all_gather(arrived, 'tp', axis=0, tiled=True)  56 us
    all_to_all x1, blocking collectives, shards(): lax.all_to_all(outgoing, SP, split_axis=0, concat_axis=0, tiled=True)  37.4 us
    all_to_all x1, blocking collectives, copy_for_each(): lax.all_to_all(jnp.broadcast_to(shard[None], (size, *shard.shape)), axis,...  19.5 us
    all_to_all x1, waiting for transfers between devices, exchange_in_order(): lax.all_to_all(blocks, axes[k], split_axis=k, concat_axis=k, tiled=True)  17.2 us
    all_to_all x1, starting transfers between devices, exchange_in_order(): lax.all_to_all(blocks, axes[k], split_axis=k, concat_axis=k, tiled=True)  12.7 us
    all_to_all x1, waiting for transfers between devices, shards(): lax.all_to_all(mixed, 'tp', split_axis=0, concat_axis=1, tiled=True)  7.6 us
    reshape x1, local copies, waits for them, and re-layouts, shards(): flat_rows = piece.reshape(-1, width)  7.21 us
  transfers between devices with their start and end apart: 4, of which 4 were waited for; matrix products, arithmetic and copies ran while one was open for 1% of the time, Pallas kernels for 0%

commit v1 on v0

v1 whole, which is shorter than its diff:
```python
import functools

import jax
import jax.numpy as jnp
from jax import lax
from jax.experimental import pallas as pl
from jax.experimental.pallas import tpu as pltpu
from jax.sharding import Mesh
from jax.sharding import PartitionSpec as P

MESH = pl.DeviceIdType.MESH
AXES = ("z", "c", "y", "x")
EPS = 1e-06
GROUPS = 4
SPAN = 16
NC = 4
STAGES = 9
ORDER = (8, 7, 6, 5, 4, 3, 2, 1, 0)
F32, BF16 = jnp.float32, jnp.bfloat16
NN = (((1,), (0,)), ((), ()))
NT = (((1,), (1,)), ((), ()))


def mm(a, b, dims=NN):
    return lax.dot_general(a, b, dims, preferred_element_type=F32)


def kernel(
    nz,
    res_any, mix_gain, pool_w, pool_scale, ffn_gain, ids, wts, gate_any, up_any, down_any,
    out,
    res, gate, up, down, ng, rim, aft, pick, code, sel, cols,
    sent, slots, part, got1, got2, got3, got4, summed, ret, normed,
    lsem, rim_s, rim_r, dsp_s, dsp_r, ret_s, ret_r, own_s, ag_s, ag_r, rs_s, rs_r, og_s, og_r,
):
    tokens, width = res.shape
    group = width // GROUPS
    experts = nz * 2
    blk = tokens * 2 // 16
    chunk = experts * blk // NC
    half, quart = chunk // 2, chunk // 4
    per = experts // NC
    z, c, y, x = (lax.axis_index(a) for a in AXES)

    def along(axis, d):
        return {axis: ({"x": x, "y": y}[axis] + d) % 4}

    barrier = pltpu.get_barrier_semaphore()
    for r in range(nz):
        for rel in range(2):
            if r or rel:
                pl.semaphore_signal(
                    barrier, 1, device_id={"z": (z + r) % nz, "c": (c + rel) % 2}, device_id_type=MESH
                )
    for axis in ("x", "y"):
        for d in (1, 3):
            pl.semaphore_signal(barrier, 1, device_id=along(axis, d), device_id_type=MESH)

    loads = [
        pltpu.make_async_copy(s, d, lsem.at[i])
        for i, (s, d) in enumerate(((res_any, res), (gate_any, gate), (up_any, up), (down_any, down)))
    ]
    for copy in loads:
        copy.start()

    window = lax.shift_left(jnp.int32(1), y + 1)
    eid = lax.broadcasted_iota(jnp.int32, (experts, tokens), 0)
    m0, m1 = ids[0:1, :] == eid, ids[1:2, :] == eid
    ti = lax.broadcasted_iota(jnp.int32, (tokens, tokens), 0)
    tj = lax.broadcasted_iota(jnp.int32, (tokens, tokens), 1)
    named = jnp.where(m0 | m1, 1.0, 0.0)
    before = mm(named.astype(BF16), jnp.where(ti < tj, 1.0, 0.0).astype(BF16))
    code[...] = jnp.where(m0 | m1, before, -1.0)
    target = eid.astype(F32) * blk + before
    t0 = jnp.sum(jnp.where(m0, target, 0.0), axis=0, keepdims=True)
    t1 = jnp.sum(jnp.where(m1, target, 0.0), axis=0, keepdims=True)
    tall = jnp.concatenate([t0, t1, wts[0:1, :], wts[1:2, :], jnp.zeros((4, tokens), F32)], axis=0)
    cols[...] = jnp.transpose(tall)
    place = lax.broadcasted_iota(jnp.int32, (blk, tokens), 0).astype(F32)
    for e in range(experts):
        pick[e * blk : (e + 1) * blk, :] = jnp.where(code[e : e + 1, :] == place, 1.0, 0.0).astype(BF16)

    loads[0].wait()
    first = pl.multiple_of(y * group, group)
    gain = mix_gain[:, pl.ds(first, group)]
    for b in range(tokens // 32):
        rows = pl.ds(b * 32, 32)
        v = res[rows, :].astype(F32)
        inv = lax.rsqrt(jnp.sum(v * v, axis=1, keepdims=True) / width + EPS)
        ng[rows, :] = (res[rows, pl.ds(first, group)].astype(F32) * inv * gain).astype(BF16)

    pl.semaphore_wait(barrier, nz * 2 + 3)
    nxt = {"z": (z + c) % nz, "c": (c + 1) % 2}
    rim_copy = pltpu.make_async_remote_copy(
        src_ref=ng.at[pl.ds(tokens - SPAN, SPAN)], dst_ref=rim, send_sem=rim_s, recv_sem=rim_r,
        device_id=nxt, device_id_type=MESH,
    )
    rim_copy.start()

    mine = pl.multiple_of((y * 4 + x) * 128, 128)
    start = (z * 2 + c) * tokens

    def mixed_rows(wsum, count):
        pos = start + lax.broadcasted_iota(jnp.int32, (count, 1), 0)
        div = jnp.minimum(pos + 1, window).astype(F32)
        pooled = (wsum / div - ng[0:count, :].astype(F32)).astype(BF16)
        mixed = (mm(pooled, pool_w[...]) * pool_scale[...]).astype(BF16).astype(F32)
        aft[0:count, :] = (res[0:count, pl.ds(mine, 128)].astype(F32) + mixed).astype(BF16)

    band = jnp.where((tj <= ti) & (tj > ti - window), 1.0, 0.0).astype(BF16)
    mixed_rows(mm(band, ng[...]), tokens)

    rim_copy.wait_recv()
    ri = lax.broadcasted_iota(jnp.int32, (SPAN, SPAN), 0)
    rj = lax.broadcasted_iota(jnp.int32, (SPAN, SPAN), 1)
    bend = jnp.where(rj <= ri, jnp.where(rj > ri - window, 1.0, 0.0), 0.0).astype(BF16)
    over = jnp.where(rj - SPAN > ri - window, 1.0, 0.0) * jnp.where(z * 2 + c > 0, 1.0, 0.0)
    mixed_rows(mm(bend, ng[0:SPAN, :]) + mm(over.astype(BF16), rim[...]), SPAN)

    sent[...] = mm(pick[...], aft[...]).astype(BF16)
    for r in range(nz):
        dz = (r + 1) // 2 if r % 2 else -(r // 2)
        for rel in range(2):
            zd, cd = (z - dz + nz) % nz, (c + rel) % 2
            src = sent.at[pl.ds(pl.multiple_of((zd * 2 + cd) * blk, blk), blk)]
            j = 2 * r + rel
            dst = slots.at[y, x, pl.ds(j * blk, blk)]
            if j:
                pltpu.make_async_remote_copy(
                    src_ref=src, dst_ref=dst, send_sem=dsp_s, recv_sem=dsp_r.at[j // per],
                    device_id={"z": zd, "c": cd}, device_id_type=MESH,
                ).start()
            else:
                pltpu.make_async_copy(src, dst, own_s.at[0]).start()

    lane = lax.broadcasted_iota(jnp.int32, (tokens, experts * blk), 1).astype(F32)
    for k in range(2):
        sel[k * tokens : (k + 1) * tokens, :] = jnp.where(cols[:, k : k + 1] == lane, 1.0, 0.0).astype(BF16)

    def landed(ref, sem):
        pltpu.make_async_copy(ref, ref, sem).wait()

    def push(src, dst, s, r, to):
        pltpu.make_async_remote_copy(
            src_ref=src, dst_ref=dst, send_sem=s, recv_sem=r, device_id=to, device_id_type=MESH
        ).start()

    DIRS = ((0, 1), (1, 3))
    HALVES = ((0, "x", "y"), (1, "y", "x"))

    def gather_stages(buf, base_of, hl, qt, ss, rs):
        def rows(k, h, off, n):
            return pl.ds(base_of(k) + h * hl + off, n)

        def one(h, d, k, off, n):
            if h == 0:
                return buf.at[y, (x + d) % 4, rows(k, h, off, n)]
            return buf.at[(y + d) % 4, x, rows(k, h, off, n)]

        def line(h, d, k, off, n):
            if h == 0:
                return buf.at[(y + d) % 4, :, rows(k, h, off, n)]
            return buf.at[:, (x + d) % 4, rows(k, h, off, n)]

        def a1(k):
            for h, ax, _ in HALVES:
                for i, d in DIRS:
                    push(one(h, 0, k, 0, hl), one(h, 0, k, 0, hl), ss.at[k, 0, h, i], rs.at[k, 0, h, i], along(ax, d))

        def a2(k):
            for h, ax, _ in HALVES:
                for i, d in DIRS:
                    landed(one(h, 4 - d, k, 0, hl), rs.at[k, 0, h, i])
                    ref = one(h, 4 - d, k, i * qt, qt)
                    push(ref, ref, ss.at[k, 1, h, i], rs.at[k, 1, h, i], along(ax, d))

        def a3(k):
            for h, _, ax in HALVES:
                for i, d in DIRS:
                    landed(one(h, 2, k, i * qt, qt), rs.at[k, 1, h, i])
                for i, d in DIRS:
                    ref = line(h, 0, k, 0, hl)
                    push(ref, ref, ss.at[k, 2, h, i], rs.at[k, 2, h, i], along(ax, d))

        def a4(k):
            for h, _, ax in HALVES:
                for i, d in DIRS:
                    landed(line(h, 4 - d, k, 0, hl), rs.at[k, 2, h, i])
                    ref = line(h, 4 - d, k, i * qt, qt)
                    push(ref, ref, ss.at[k, 3, h, i], rs.at[k, 3, h, i], along(ax, d))

        def a5(k):
            for h, _, _ in HALVES:
                for i, d in DIRS:
                    landed(line(h, 2, k, i * qt, qt), rs.at[k, 3, h, i])

        def drain(k):
            for h in (0, 1):
                for i in (0, 1):
                    for st, ref in enumerate(
                        (one(h, 0, k, 0, hl), one(h, 0, k, 0, qt), line(h, 0, k, 0, hl), line(h, 0, k, 0, qt))
                    ):
                        landed(ref, ss.at[k, st, h, i])

        return a1, a2, a3, a4, a5, drain

    def base_of(k):
        return pl.multiple_of(k * chunk, chunk)

    a1, a2, a3, a4, a5, ag_drain = gather_stages(slots, base_of, half, quart, ag_s, ag_r)

    def s0(k):
        @pl.when(k == 0)
        def _():
            landed(slots.at[y, x, pl.ds(0, blk)], own_s.at[0])
            landed(slots.at[y, x, pl.ds(blk, chunk - blk)], dsp_r.at[0])

        @pl.when(k > 0)
        def _():
            landed(slots.at[y, x, pl.ds(base_of(k), chunk)], dsp_r.at[k])

        a1(k)

    def line(h, d, k, off, n):
        rows = pl.ds(base_of(k) + h * half + off, n)
        if h == 0:
            return part.at[(y + d) % 4, :, rows]
        return part.at[:, (x + d) % 4, rows]

    def one(h, d, k, off, n):
        rows = pl.ds(base_of(k) + h * half + off, n)
        if h == 0:
            return part.at[y, (x + d) % 4, rows]
        return part.at[(y + d) % 4, x, rows]

    SUMS = ((0, "y", "x"), (1, "x", "y"))

    def ffn(k):
        a5(k)

        @pl.when(k == 0)
        def _():
            for copy in loads[1:]:
                copy.wait()

        def norm(b, carry):
            rows = pl.ds(pl.multiple_of(base_of(k) + b * 32, 32), 32)
            total = jnp.zeros((32, 128), F32)
            for t in range(16):
                v = slots[t // 4, t % 4, rows, :].astype(F32)
                total = total + v * v
            inv = lax.rsqrt(jnp.sum(total, axis=1, keepdims=True) / width + EPS)
            put = pl.ds(pl.multiple_of(b * 32, 32), 32)
            for t in range(16):
                v = slots[t // 4, t % 4, rows, :].astype(F32)
                normed[put, t * 128 : (t + 1) * 128] = (
                    v * inv * ffn_gain[:, t * 128 : (t + 1) * 128]
                ).astype(BF16)
            return carry

        lax.fori_loop(0, chunk // 32, norm, 0)
        g = mm(normed[...], gate[...], NT)
        u = mm(normed[...], up[...], NT)
        hidden = (jax.nn.silu(g) * u).astype(BF16)
        rows = pl.ds(base_of(k), chunk)
        for t in range(0, 16, 2):
            p = mm(hidden, down[:, t * 128 : (t + 2) * 128]).astype(BF16)
            part[t // 4, t % 4, rows, :] = p[:, :128]
            part[t // 4, t % 4 + 1, rows, :] = p[:, 128:]
        for h, ax, _ in SUMS:
            for i, d in DIRS:
                push(line(h, 2, k, i * quart, quart), got1.at[k, h, i], rs_s.at[k, 0, h, i], rs_r.at[k, 0, h, i], along(ax, d))

    def add(ref, *others):
        total = ref[...].astype(F32)
        for other in others:
            total = total + other[...].astype(F32)
        ref[...] = total.astype(BF16)

    def r2(k):
        for h, ax, _ in SUMS:
            for i, d in DIRS:
                landed(got1.at[k, h, i], rs_r.at[k, 0, h, i])
                add(line(h, d, k, i * quart, quart), got1.at[k, h, i])
                push(line(h, d, k, 0, half), got2.at[k, h, i], rs_s.at[k, 1, h, i], rs_r.at[k, 1, h, i], along(ax, d))

    def r3(k):
        for h, _, ax in SUMS:
            for i, d in DIRS:
                landed(got2.at[k, h, i], rs_r.at[k, 1, h, i])
            add(line(h, 0, k, 0, half), got2.at[k, h, 0], got2.at[k, h, 1])
            for i, d in DIRS:
                push(one(h, 2, k, i * quart, quart), got3.at[k, h, i], rs_s.at[k, 2, h, i], rs_r.at[k, 2, h, i], along(ax, d))

    def r4(k):
        for h, _, ax in SUMS:
            for i, d in DIRS:
                landed(got3.at[k, h, i], rs_r.at[k, 2, h, i])
                add(one(h, d, k, i * quart, quart), got3.at[k, h, i])
                push(one(h, d, k, 0, half), got4.at[k, h, i], rs_s.at[k, 3, h, i], rs_r.at[k, 3, h, i], along(ax, d))

    home = pl.ds(pl.multiple_of((z * 2 + c) * blk, blk), blk)

    def back(k):
        for h, _, _ in SUMS:
            for i, d in DIRS:
                landed(got4.at[k, h, i], rs_r.at[k, 3, h, i])
            total = one(h, 0, k, 0, half)[...].astype(F32)
            total = total + got4[k, h, 0].astype(F32) + got4[k, h, 1].astype(F32)
            summed[pl.ds(base_of(k) + h * half, half), :] = total.astype(BF16)
        for i in range(per):
            r = k * (per // 2) + i // 2
            dz = (r % 2) * ((r + 1) // 2) + (1 - r % 2) * (nz - r // 2)
            src = summed.at[pl.ds(pl.multiple_of(base_of(k) + i * blk, blk), blk)]
            to = {"z": (z + dz) % nz, "c": (c + i % 2) % 2}
            if i == 0:

                @pl.when(k == 0)
                def _():
                    pltpu.make_async_copy(src, ret.at[home], own_s.at[1]).start()

                @pl.when(k > 0)
                def _():
                    push(src, ret.at[home], ret_s, ret_r, to)
            else:
                push(src, ret.at[home], ret_s, ret_r, to)

    def rs_drain(k):
        for h in (0, 1):
            for i in (0, 1):
                for st, ref in enumerate((got1, got2, got3, got4)):
                    landed(ref.at[k, h, i], rs_s.at[k, st, h, i])

    stages = (s0, a2, a3, a4, ffn, r2, r3, r4, back)

    def step(tau, carry):
        for s in ORDER:
            k = tau - s

            @pl.when((k >= 0) & (k < NC))
            def _(s=s, k=k):
                stages[s](k)

        return carry

    lax.fori_loop(0, NC + STAGES - 1, step, 0)

    landed(ret.at[pl.ds(0, blk)], own_s.at[1])
    landed(ret.at[pl.ds(blk, (experts - 1) * blk)], ret_r)
    picked = mm(sel[...], ret[...])
    mix = cols[:, 2:3] * picked[:tokens] + cols[:, 3:4] * picked[tokens:]
    out[y, x, :, :] = (aft[...].astype(F32) + mix).astype(BF16)
    o1, o2, o3, o4, o5, og_drain = gather_stages(out, lambda k: 0, tokens // 2, tokens // 4, og_s, og_r)
    for stage in (o1, o2, o3, o4, o5):
        stage(0)

    rim_copy.wait_send()
    landed(sent.at[pl.ds(0, (experts - 1) * blk)], dsp_s)
    landed(summed.at[pl.ds(0, (experts - 1) * blk)], ret_s)

    def drains(k, carry):
        ag_drain(k)
        rs_drain(k)
        return carry

    lax.fori_loop(0, NC, drains, 0)
    og_drain(0)


def shards(res, mix_gain, pool_w, pool_scale, ffn_gain, ids, wts, gate, up, down):
    nz = lax.axis_size("z")
    tokens, width = res.shape
    ff = gate.shape[2]
    experts = nz * 2
    blk = tokens * 2 // 16
    total = experts * blk
    chunk = total // NC
    vmem, hbm = pl.BlockSpec(memory_space=pltpu.VMEM), pl.BlockSpec(memory_space=pl.ANY)
    dma, V = pltpu.SemaphoreType.DMA, pltpu.VMEM
    out = pl.pallas_call(
        functools.partial(kernel, nz),
        name="layer",
        out_shape=jax.ShapeDtypeStruct((4, 4, tokens, 128), BF16),
        in_specs=[hbm, vmem, vmem, vmem, vmem, vmem, vmem, hbm, hbm, hbm],
        out_specs=vmem,
        scratch_shapes=[
            V((tokens, width), BF16),
            V((ff, width), BF16),
            V((ff, width), BF16),
            V((ff, width), BF16),
            V((tokens, width // GROUPS), BF16),
            V((SPAN, width // GROUPS), BF16),
            V((tokens, 128), BF16),
            V((total, tokens), BF16),
            V((experts, tokens), F32),
            V((2 * tokens, total), BF16),
            V((tokens, 8), F32),
            V((total, 128), BF16),
            V((4, 4, total, 128), BF16),
            V((4, 4, total, 128), BF16),
            V((NC, 2, 2, 4, chunk // 4, 128), BF16),
            V((NC, 2, 2, 4, chunk // 2, 128), BF16),
            V((NC, 2, 2, chunk // 4, 128), BF16),
            V((NC, 2, 2, chunk // 2, 128), BF16),
            V((total, 128), BF16),
            V((total, 128), BF16),
            V((chunk, width), BF16),
            dma((4,)),
            dma, dma, dma, dma((NC,)), dma, dma, dma((2,)),
            dma((NC, 4, 2, 2)), dma((NC, 4, 2, 2)), dma((NC, 4, 2, 2)), dma((NC, 4, 2, 2)),
            dma((1, 4, 2, 2)), dma((1, 4, 2, 2)),
        ],
        compiler_params=pltpu.CompilerParams(
            collective_id=0, has_side_effects=True, vmem_limit_bytes=60 * 1024 * 1024
        ),
    )(
        res, mix_gain.reshape(1, -1), pool_w, pool_scale.reshape(1, -1), ffn_gain.reshape(1, -1),
        ids.T, wts.T, gate[0].T, up[0].T, down[0],
    )
    return jnp.transpose(out.reshape(16, tokens, 128), (1, 0, 2)).reshape(tokens, width)


def solution(mesh):
    torus = Mesh(mesh.devices.reshape(mesh.shape["sp"] // 2, 2, 4, 4), AXES)
    sp, tp = ("z", "c"), ("y", "x")
    return jax.shard_map(
        shards,
        mesh=torus,
        in_specs=(
            P(sp, None),
            P(),
            P(None, tp),
            P(tp),
            P(),
            P(sp, None),
            P(sp, None),
            P(sp, None, tp),
            P(sp, None, tp),
            P(sp, tp, None),
        ),
        out_specs=P(sp, None),
        check_vma=False,
    )
```

time: 269 us -> 114 us (0.42)
  blocking collectives: 117 us -> 0 us
  Pallas kernels: 0 us -> 111 us
  waiting for transfers between devices: 83.3 us -> 0 us
  starting transfers between devices: 21.7 us -> 0 us
  matrix products: 14.4 us -> 0 us
  between operations: 13.7 us -> 0.01 us
  local copies, waits for them, and re-layouts: 12 us -> 2.49 us
  other arithmetic: 6.75 us -> 0 us
    all_to_all x4 -> x0, blocking collectives: 117 us -> none  [the longest x1 56 us: sent_and_summed(): blocks = lax.all_to_all(split_up(shard, dim, size), axis, 0, 0, tiled=True)]
    pallas_call x0 -> x1, Pallas kernels: none -> 111 us  [shards(): pl.pallas_call(functools.partial(kernel, nz), name='layer', out_shape=jax...]
    all_gather x1 -> x0, waiting for transfers between devices: 56 us -> none  [shards(): piece = lax.all_gather(arrived, 'tp', axis=0, tiled=True)]
    all_to_all x2 -> x0, waiting for transfers between devices: 24.8 us -> none  [the longest x1 17.2 us: exchange_in_order(): lax.all_to_all(blocks, axes[k], split_axis=k, concat_axis=k, tiled=True)]
    all_to_all x2 -> x0, starting transfers between devices: 19.7 us -> none  [the longest x1 12.7 us: exchange_in_order(): lax.all_to_all(blocks, axes[k], split_axis=k, concat_axis=k, tiled=True)]
    dot_general x6 -> x0, matrix products: 14.4 us -> none  [the longest x1 7 us: shards(): jnp.dot(hidden_flat, down_weight[0], preferred_element_type=jnp.float32)]
    reshape x3 -> x1, local copies, waits for them, and re-layouts: 7.45 us -> 2.49 us  [shards(): jnp.transpose(out.reshape(16, tokens, 128), (1, 0, 2))]
    reduce_sum x4 -> x0, other arithmetic: 4.89 us -> none  [the longest x1 2.98 us: sent_and_summed(): return jnp.sum(blocks.astype(jnp.float32), axis=0)]
  transfers between devices with their start and end apart: 4 -> 0, of which waited for: 4 -> 0; matrix products, arithmetic and copies ran while one was open for 1% -> 0% of each run, Pallas kernels for 0% -> 0%
where the time goes in v1:
time: 114 us
  Pallas kernels  111 us (97%)
  local copies, waits for them, and re-layouts  2.49 us (2%)
    pallas_call x1, Pallas kernels, shards(): pl.pallas_call(functools.partial(kernel, nz), name='layer', out_shape=jax...  111 us
    reshape x1, local copies, waits for them, and re-layouts, shards(): jnp.transpose(out.reshape(16, tokens, 128), (1, 0, 2))  2.49 us

profile of v1, /device:TPU:32, one launch (start us, length us, event | category | flops | bytes accessed | tf_op | source)
XLA Modules:
  0.0 113.8 jit_solution(16906219446455163374)
XLA Ops:
  0.0 111.3 %layer.1 = bf16[4,4,256,128]{3,2,1,0:T(8,128)(2,1)} custom-call(bf16[256,2048]{1,0:T(8,128)(2,1)} %res_any.1, f32[1,2048]{1,0:T(1,128)} %bitcast.23, bf16[512,128]{1,0:T(8,128)(2,1)} %pool_w.1, f32[1,128]{1,0:T(1,128)} %bitcast.27, f32[1,2048]{1,0:T(1,128)} %bitcast.24, s32[2,256]{1,0:T(2,128)} %bitcast.25, f32[2,256]{1,0:T(2,128)} %bitcast.26, ...), custom_call_target="tpu_custom_call" | custom-call | tf_op jit(solution)/shard_map/layer/pallas_call | solution.py:380
  111.3 2.5 %copy.14 = bf16[16,32,8,128]{3,2,0,1:T(8,128)(2,1)} copy(bf16[16,32,8,128]{3,2,1,0:T(8,128)(2,1)} %bitcast.19) | data formatting | bytes 2097152 | tf_op jit(solution)/shard_map/reshape | solution.py:420

commit v2 on v1

--- a/solution.py
+++ b/solution.py
@@ -14,8 +14,11 @@
 GROUPS = 4
 SPAN = 16
 NC = 4
-STAGES = 9
-ORDER = (8, 7, 6, 5, 4, 3, 2, 1, 0)
+ORDER = (0, 1, 2, 3, 4, 5, 6)
+NO = 2
+DZ = (0, 1, -1, 2, -4, 5, -5, 6, -6, 7, -7, 8, -2, 3, -3, 4)
+TOKENS = True
+SPLIT = 2
 F32, BF16 = jnp.float32, jnp.bfloat16
 NN = (((1,), (0,)), ((), ()))
 NT = (((1,), (1,)), ((), ()))
@@ -28,10 +31,10 @@
 def kernel(
     nz,
     res_any, mix_gain, pool_w, pool_scale, ffn_gain, ids, wts, gate_any, up_any, down_any,
-    out,
+    out_any,
     res, gate, up, down, ng, rim, aft, pick, code, sel, cols,
-    sent, slots, part, got1, got2, got3, got4, summed, ret, normed,
-    lsem, rim_s, rim_r, dsp_s, dsp_r, ret_s, ret_r, own_s, ag_s, ag_r, rs_s, rs_r, og_s, og_r,
+    sent, slots, part, got1, got2, got3, summed, ret, normed, out,
+    lsem, rim_s, rim_r, dsp_s, dsp_r, ret_s, ret_r, own_s, ag_s, ag_r, rs_s, rs_r, og_s, og_r, out_s, tokp, tokm,
 ):
     tokens, width = res.shape
     group = width // GROUPS
@@ -46,14 +49,15 @@
         return {axis: ({"x": x, "y": y}[axis] + d) % 4}
 
     barrier = pltpu.get_barrier_semaphore()
-    for r in range(nz):
+    reach = (0, 1, nz - 1) if TOKENS else range(nz)
+    for r in reach:
         for rel in range(2):
             if r or rel:
                 pl.semaphore_signal(
                     barrier, 1, device_id={"z": (z + r) % nz, "c": (c + rel) % 2}, device_id_type=MESH
                 )
     for axis in ("x", "y"):
-        for d in (1, 3):
+        for d in (1, 2, 3):
             pl.semaphore_signal(barrier, 1, device_id=along(axis, d), device_id_type=MESH)
 
     loads = [
@@ -63,7 +67,28 @@
     for copy in loads:
         copy.start()
 
+    def pass_on(h):
+        if not TOKENS:
+            return
+        if h > 1:
+            pl.semaphore_wait(tokp.at[h], 1)
+            if h < nz // 2:
+                pl.semaphore_wait(tokm.at[h], 1)
+        if h < nz // 2:
+            pl.semaphore_signal(tokp.at[h + 1], 1, device_id={"z": (z + 1) % nz}, device_id_type=MESH)
+        if h < nz // 2 - 1:
+            pl.semaphore_signal(tokm.at[h + 1], 1, device_id={"z": (z + nz - 1) % nz}, device_id_type=MESH)
+
     window = lax.shift_left(jnp.int32(1), y + 1)
+    first = pl.multiple_of(y * group, group)
+    gain = mix_gain[:, pl.ds(first, group)]
+
+    def norm_rows(at, n):
+        rows = pl.ds(at, n)
+        v = res[rows, :].astype(F32)
+        inv = lax.rsqrt(jnp.sum(v * v, axis=1, keepdims=True) / width + EPS)
+        ng[rows, :] = (res[rows, pl.ds(first, group)].astype(F32) * inv * gain).astype(BF16)
+
     eid = lax.broadcasted_iota(jnp.int32, (experts, tokens), 0)
     m0, m1 = ids[0:1, :] == eid, ids[1:2, :] == eid
     ti = lax.broadcasted_iota(jnp.int32, (tokens, tokens), 0)
@@ -77,25 +102,21 @@
     tall = jnp.concatenate([t0, t1, wts[0:1, :], wts[1:2, :], jnp.zeros((4, tokens), F32)], axis=0)
     cols[...] = jnp.transpose(tall)
     place = lax.broadcasted_iota(jnp.int32, (blk, tokens), 0).astype(F32)
-    for e in range(experts):
-        pick[e * blk : (e + 1) * blk, :] = jnp.where(code[e : e + 1, :] == place, 1.0, 0.0).astype(BF16)
 
     loads[0].wait()
-    first = pl.multiple_of(y * group, group)
-    gain = mix_gain[:, pl.ds(first, group)]
-    for b in range(tokens // 32):
-        rows = pl.ds(b * 32, 32)
-        v = res[rows, :].astype(F32)
-        inv = lax.rsqrt(jnp.sum(v * v, axis=1, keepdims=True) / width + EPS)
-        ng[rows, :] = (res[rows, pl.ds(first, group)].astype(F32) * inv * gain).astype(BF16)
-
-    pl.semaphore_wait(barrier, nz * 2 + 3)
+    norm_rows(tokens - 32, 32)
+    pl.semaphore_wait(barrier, 11 if TOKENS else nz * 2 + 5)
     nxt = {"z": (z + c) % nz, "c": (c + 1) % 2}
     rim_copy = pltpu.make_async_remote_copy(
         src_ref=ng.at[pl.ds(tokens - SPAN, SPAN)], dst_ref=rim, send_sem=rim_s, recv_sem=rim_r,
         device_id=nxt, device_id_type=MESH,
     )
     rim_copy.start()
+    pass_on(1)
+
+    for b in range(tokens // 32 - 1):
+        norm_rows(b * 32, 32)
+    pass_on(2)
 
     mine = pl.multiple_of((y * 4 + x) * 128, 128)
     start = (z * 2 + c) * tokens
@@ -109,6 +130,9 @@
 
     band = jnp.where((tj <= ti) & (tj > ti - window), 1.0, 0.0).astype(BF16)
     mixed_rows(mm(band, ng[...]), tokens)
+    for e in range(experts):
+        pick[e * blk : (e + 1) * blk, :] = jnp.where(code[e : e + 1, :] == place, 1.0, 0.0).astype(BF16)
+    pass_on(3)
 
     rim_copy.wait_recv()
     ri = lax.broadcasted_iota(jnp.int32, (SPAN, SPAN), 0)
@@ -118,10 +142,13 @@
     mixed_rows(mm(bend, ng[0:SPAN, :]) + mm(over.astype(BF16), rim[...]), SPAN)
 
     sent[...] = mm(pick[...], aft[...]).astype(BF16)
-    for r in range(nz):
-        dz = (r + 1) // 2 if r % 2 else -(r // 2)
+    known = 3
+    for r, dz in enumerate(DZ):
+        while known < abs(dz):
+            known += 1
+            pass_on(known)
         for rel in range(2):
-            zd, cd = (z - dz + nz) % nz, (c + rel) % 2
+            zd, cd = (z + (nz - dz) % nz) % nz, (c + rel) % 2
             src = sent.at[pl.ds(pl.multiple_of((zd * 2 + cd) * blk, blk), blk)]
             j = 2 * r + rel
             dst = slots.at[y, x, pl.ds(j * blk, blk)]
@@ -148,7 +175,11 @@
     DIRS = ((0, 1), (1, 3))
     HALVES = ((0, "x", "y"), (1, "y", "x"))
 
-    def gather_stages(buf, base_of, hl, qt, ss, rs):
+    def pieces(hl):
+        cut = hl * SPLIT // 4
+        return ((0, 1, 0, cut), (1, 3, cut, hl - cut))
+
+    def gather_stages(buf, base_of, hl, ss, rs):
         def rows(k, h, off, n):
             return pl.ds(base_of(k) + h * hl + off, n)
 
@@ -163,51 +194,44 @@
             return buf.at[:, (x + d) % 4, rows(k, h, off, n)]
 
         def a1(k):
-            for h, ax, _ in HALVES:
+            for d in (1, 3, 2):
+                for h, ax, _ in HALVES:
+                    push(one(h, 0, k, 0, hl), one(h, 0, k, 0, hl), ss.at[k, 0, h, d - 1], rs.at[k, 0, h, d - 1], along(ax, d))
+
+        def a2(k):
+            for h, _, ax in HALVES:
+                for d in (1, 3, 2):
+                    landed(one(h, 4 - d, k, 0, hl), rs.at[k, 0, h, d - 1])
                 for i, d in DIRS:
-                    push(one(h, 0, k, 0, hl), one(h, 0, k, 0, hl), ss.at[k, 0, h, i], rs.at[k, 0, h, i], along(ax, d))
-
-        def a2(k):
-            for h, ax, _ in HALVES:
-                for i, d in DIRS:
-                    landed(one(h, 4 - d, k, 0, hl), rs.at[k, 0, h, i])
-                    ref = one(h, 4 - d, k, i * qt, qt)
+                    ref = line(h, 0, k, 0, hl)
                     push(ref, ref, ss.at[k, 1, h, i], rs.at[k, 1, h, i], along(ax, d))
 
         def a3(k):
             for h, _, ax in HALVES:
-                for i, d in DIRS:
-                    landed(one(h, 2, k, i * qt, qt), rs.at[k, 1, h, i])
-                for i, d in DIRS:
-                    ref = line(h, 0, k, 0, hl)
+                for i, d, off, n in pieces(hl):
+                    landed(line(h, 4 - d, k, 0, hl), rs.at[k, 1, h, i])
+                    ref = line(h, 4 - d, k, off, n)
                     push(ref, ref, ss.at[k, 2, h, i], rs.at[k, 2, h, i], along(ax, d))
 
         def a4(k):
-            for h, _, ax in HALVES:
-                for i, d in DIRS:
-                    landed(line(h, 4 - d, k, 0, hl), rs.at[k, 2, h, i])
-                    ref = line(h, 4 - d, k, i * qt, qt)
-                    push(ref, ref, ss.at[k, 3, h, i], rs.at[k, 3, h, i], along(ax, d))
-
-        def a5(k):
             for h, _, _ in HALVES:
-                for i, d in DIRS:
-                    landed(line(h, 2, k, i * qt, qt), rs.at[k, 3, h, i])
+                for i, d, off, n in pieces(hl):
+                    landed(line(h, 2, k, off, n), rs.at[k, 2, h, i])
 
         def drain(k):
             for h in (0, 1):
-                for i in (0, 1):
-                    for st, ref in enumerate(
-                        (one(h, 0, k, 0, hl), one(h, 0, k, 0, qt), line(h, 0, k, 0, hl), line(h, 0, k, 0, qt))
-                    ):
-                        landed(ref, ss.at[k, st, h, i])
-
-        return a1, a2, a3, a4, a5, drain
+                for d in (1, 2, 3):
+                    landed(one(h, 0, k, 0, hl), ss.at[k, 0, h, d - 1])
+                for i, _, off, n in pieces(hl):
+                    landed(line(h, 0, k, 0, hl), ss.at[k, 1, h, i])
+                    landed(line(h, 0, k, 0, n), ss.at[k, 2, h, i])
+
+        return a1, a2, a3, a4, drain
 
     def base_of(k):
         return pl.multiple_of(k * chunk, chunk)
 
-    a1, a2, a3, a4, a5, ag_drain = gather_stages(slots, base_of, half, quart, ag_s, ag_r)
+    a1, a2, a3, a4, ag_drain = gather_stages(slots, base_of, half, ag_s, ag_r)
 
     def s0(k):
         @pl.when(k == 0)
@@ -236,7 +260,7 @@
     SUMS = ((0, "y", "x"), (1, "x", "y"))
 
     def ffn(k):
-        a5(k)
+        a4(k)
 
         @pl.when(k == 0)
         def _():
@@ -268,8 +292,8 @@
             part[t // 4, t % 4, rows, :] = p[:, :128]
             part[t // 4, t % 4 + 1, rows, :] = p[:, 128:]
         for h, ax, _ in SUMS:
-            for i, d in DIRS:
-                push(line(h, 2, k, i * quart, quart), got1.at[k, h, i], rs_s.at[k, 0, h, i], rs_r.at[k, 0, h, i], along(ax, d))
+            for i, d, off, n in pieces(half):
+                push(line(h, 2, k, off, n), got1.at[k, h, :, pl.ds(off, n)], rs_s.at[k, 0, h, i], rs_r.at[k, 0, h, i], along(ax, d))
 
     def add(ref, *others):
         total = ref[...].astype(F32)
@@ -279,9 +303,9 @@
 
     def r2(k):
         for h, ax, _ in SUMS:
-            for i, d in DIRS:
-                landed(got1.at[k, h, i], rs_r.at[k, 0, h, i])
-                add(line(h, d, k, i * quart, quart), got1.at[k, h, i])
+            for i, d, off, n in pieces(half):
+                landed(got1.at[k, h, :, pl.ds(off, n)], rs_r.at[k, 0, h, i])
+                add(line(h, d, k, off, n), got1.at[k, h, :, pl.ds(off, n)])
                 push(line(h, d, k, 0, half), got2.at[k, h, i], rs_s.at[k, 1, h, i], rs_r.at[k, 1, h, i], along(ax, d))
 
     def r3(k):
@@ -289,49 +313,41 @@
             for i, d in DIRS:
                 landed(got2.at[k, h, i], rs_r.at[k, 1, h, i])
             add(line(h, 0, k, 0, half), got2.at[k, h, 0], got2.at[k, h, 1])
-            for i, d in DIRS:
-                push(one(h, 2, k, i * quart, quart), got3.at[k, h, i], rs_s.at[k, 2, h, i], rs_r.at[k, 2, h, i], along(ax, d))
-
-    def r4(k):
-        for h, _, ax in SUMS:
-            for i, d in DIRS:
-                landed(got3.at[k, h, i], rs_r.at[k, 2, h, i])
-                add(one(h, d, k, i * quart, quart), got3.at[k, h, i])
-                push(one(h, d, k, 0, half), got4.at[k, h, i], rs_s.at[k, 3, h, i], rs_r.at[k, 3, h, i], along(ax, d))
+            for d in (2, 1, 3):
+                push(one(h, d, k, 0, half), got3.at[k, h, d - 1], rs_s.at[k, 2, h, d - 1], rs_r.at[k, 2, h, d - 1], along(ax, d))
 
     home = pl.ds(pl.multiple_of((z * 2 + c) * blk, blk), blk)
 
     def back(k):
         for h, _, _ in SUMS:
-            for i, d in DIRS:
-                landed(got4.at[k, h, i], rs_r.at[k, 3, h, i])
+            for d in (1, 3, 2):
+                landed(got3.at[k, h, d - 1], rs_r.at[k, 2, h, d - 1])
             total = one(h, 0, k, 0, half)[...].astype(F32)
-            total = total + got4[k, h, 0].astype(F32) + got4[k, h, 1].astype(F32)
+            for d in (1, 2, 3):
+                total = total + got3[k, h, d - 1].astype(F32)
             summed[pl.ds(base_of(k) + h * half, half), :] = total.astype(BF16)
-        for i in range(per):
-            r = k * (per // 2) + i // 2
-            dz = (r % 2) * ((r + 1) // 2) + (1 - r % 2) * (nz - r // 2)
-            src = summed.at[pl.ds(pl.multiple_of(base_of(k) + i * blk, blk), blk)]
-            to = {"z": (z + dz) % nz, "c": (c + i % 2) % 2}
-            if i == 0:
-
-                @pl.when(k == 0)
-                def _():
-                    pltpu.make_async_copy(src, ret.at[home], own_s.at[1]).start()
-
-                @pl.when(k > 0)
-                def _():
-                    push(src, ret.at[home], ret_s, ret_r, to)
-            else:
-                push(src, ret.at[home], ret_s, ret_r, to)
+        for kk in range(NC):
+
+            @pl.when(k == kk)
+            def _(kk=kk):
+                for i in range(per):
+                    j = kk * per + i
+                    src = summed.at[pl.ds(j * blk, blk)]
+                    to = {"z": (z + (DZ[j // 2] + nz) % nz) % nz, "c": (c + j % 2) % 2}
+                    if j:
+                        push(src, ret.at[home], ret_s, ret_r, to)
+                    else:
+                        pltpu.make_async_copy(src, ret.at[home], own_s.at[1]).start()
 
     def rs_drain(k):
         for h in (0, 1):
-            for i in (0, 1):
-                for st, ref in enumerate((got1, got2, got3, got4)):
-                    landed(ref.at[k, h, i], rs_s.at[k, st, h, i])
-
-    stages = (s0, a2, a3, a4, ffn, r2, r3, r4, back)
+            for i, _, off, n in pieces(half):
+                landed(got1.at[k, h, :, pl.ds(off, n)], rs_s.at[k, 0, h, i])
+                landed(got2.at[k, h, i], rs_s.at[k, 1, h, i])
+            for d in (1, 2, 3):
+                landed(got3.at[k, h, d - 1], rs_s.at[k, 2, h, d - 1])
+
+    stages = (s0, a2, a3, ffn, r2, r3, back)
 
     def step(tau, carry):
         for s in ORDER:
@@ -343,16 +359,25 @@
 
         return carry
 
-    lax.fori_loop(0, NC + STAGES - 1, step, 0)
+    lax.fori_loop(0, NC + len(stages) - 1, step, 0)
 
     landed(ret.at[pl.ds(0, blk)], own_s.at[1])
     landed(ret.at[pl.ds(blk, (experts - 1) * blk)], ret_r)
     picked = mm(sel[...], ret[...])
     mix = cols[:, 2:3] * picked[:tokens] + cols[:, 3:4] * picked[tokens:]
     out[y, x, :, :] = (aft[...].astype(F32) + mix).astype(BF16)
-    o1, o2, o3, o4, o5, og_drain = gather_stages(out, lambda k: 0, tokens // 2, tokens // 4, og_s, og_r)
-    for stage in (o1, o2, o3, o4, o5):
-        stage(0)
+    oc = tokens // NO
+    *over_out, og_drain = gather_stages(out, lambda k: k * oc, oc // 2, og_s, og_r)
+    for tau in range(NO + 3):
+        for s, stage in enumerate(over_out):
+            if 0 <= tau - s < NO:
+                stage(tau - s)
+    puts = [
+        pltpu.make_async_copy(out.at[t // 4, t % 4], out_any.at[:, pl.ds(t * 128, 128)], out_s.at[t])
+        for t in range(16)
+    ]
+    for copy in puts:
+        copy.start()
 
     rim_copy.wait_send()
     landed(sent.at[pl.ds(0, (experts - 1) * blk)], dsp_s)
@@ -364,7 +389,10 @@
         return carry
 
     lax.fori_loop(0, NC, drains, 0)
-    og_drain(0)
+    for k in range(NO):
+        og_drain(k)
+    for copy in puts:
+        copy.wait()
 
 
 def shards(res, mix_gain, pool_w, pool_scale, ffn_gain, ids, wts, gate, up, down):
@@ -380,9 +408,9 @@
     out = pl.pallas_call(
         functools.partial(kernel, nz),
         name="layer",
-        out_shape=jax.ShapeDtypeStruct((4, 4, tokens, 128), BF16),
+        out_shape=jax.ShapeDtypeStruct((tokens, width), BF16),
         in_specs=[hbm, vmem, vmem, vmem, vmem, vmem, vmem, hbm, hbm, hbm],
-        out_specs=vmem,
+        out_specs=hbm,
         scratch_shapes=[
             V((tokens, width), BF16),
             V((ff, width), BF16),
@@ -398,17 +426,18 @@
             V((total, 128), BF16),
             V((4, 4, total, 128), BF16),
             V((4, 4, total, 128), BF16),
-            V((NC, 2, 2, 4, chunk // 4, 128), BF16),
+            V((NC, 2, 4, chunk // 2, 128), BF16),
             V((NC, 2, 2, 4, chunk // 2, 128), BF16),
-            V((NC, 2, 2, chunk // 4, 128), BF16),
-            V((NC, 2, 2, chunk // 2, 128), BF16),
+            V((NC, 2, 3, chunk // 2, 128), BF16),
             V((total, 128), BF16),
             V((total, 128), BF16),
             V((chunk, width), BF16),
+            V((4, 4, tokens, 128), BF16),
             dma((4,)),
             dma, dma, dma, dma((NC,)), dma, dma, dma((2,)),
-            dma((NC, 4, 2, 2)), dma((NC, 4, 2, 2)), dma((NC, 4, 2, 2)), dma((NC, 4, 2, 2)),
-            dma((1, 4, 2, 2)), dma((1, 4, 2, 2)),
+            dma((NC, 3, 2, 3)), dma((NC, 3, 2, 3)), dma((NC, 3, 2, 3)), dma((NC, 3, 2, 3)),
+            dma((NO, 3, 2, 3)), dma((NO, 3, 2, 3)), dma((16,)),
+            pltpu.SemaphoreType.REGULAR((9,)), pltpu.SemaphoreType.REGULAR((9,)),
         ],
         compiler_params=pltpu.CompilerParams(
             collective_id=0, has_side_effects=True, vmem_limit_bytes=60 * 1024 * 1024
@@ -417,7 +446,7 @@
         res, mix_gain.reshape(1, -1), pool_w, pool_scale.reshape(1, -1), ffn_gain.reshape(1, -1),
         ids.T, wts.T, gate[0].T, up[0].T, down[0],
     )
-    return jnp.transpose(out.reshape(16, tokens, 128), (1, 0, 2)).reshape(tokens, width)
+    return out
 
 
 def solution(mesh):

time: 114 us -> 105 us (0.921)
  Pallas kernels: 111 us -> 103 us
    pallas_call x1, Pallas kernels: 111 us -> 103 us  [shards(): pl.pallas_call(functools.partial(kernel, nz), name='layer', out_shape=jax...]
    reshape x1 -> x0, local copies, waits for them, and re-layouts: 2.49 us -> none  [shards(): jnp.transpose(out.reshape(16, tokens, 128), (1, 0, 2))]
    unnamed x0 -> x1, local copies, waits for them, and re-layouts: none -> 2.3 us
where the time goes in v2:
time: 105 us
  Pallas kernels  103 us (98%)
  local copies, waits for them, and re-layouts  2.3 us (2%)
    pallas_call x1, Pallas kernels, shards(): pl.pallas_call(functools.partial(kernel, nz), name='layer', out_shape=jax...  103 us
    unnamed x1, local copies, waits for them, and re-layouts  2.3 us

profile of v2, /device:TPU:32, one launch (start us, length us, event | category | flops | bytes accessed | tf_op | source)
XLA Modules:
  0.0 105.0 jit_solution(18433264114424839152)
XLA Ops:
  0.0 102.6 %layer.1 = bf16[256,2048]{1,0:T(8,128)(2,1)} custom-call(bf16[256,2048]{1,0:T(8,128)(2,1)} %res_any.1, f32[1,2048]{1,0:T(1,128)} %bitcast.15, bf16[512,128]{1,0:T(8,128)(2,1)} %pool_w.1, f32[1,128]{1,0:T(1,128)} %bitcast.19, f32[1,2048]{1,0:T(1,128)} %bitcast.16, s32[2,256]{1,0:T(2,128)} %bitcast.17, f32[2,256]{1,0:T(2,128)} %bitcast.18, ...), custom_call_target="tpu_custom_call" | custom-call | tf_op jit(solution)/shard_map/layer/pallas_call | solution.py:408
  102.7 2.3 %copy.12 = bf16[256,2048]{1,0:T(8,128)(2,1)} copy(bf16[256,2048]{1,0:T(8,128)(2,1)} %layer.1) | data formatting | bytes 2097152

commit v3 on v2

--- a/solution.py
+++ b/solution.py
@@ -14,10 +14,9 @@
 GROUPS = 4
 SPAN = 16
 NC = 4
-ORDER = (0, 1, 2, 3, 4, 5, 6)
+ORDER = (2, 1, 0, 3, 4, 5, 6)
 NO = 2
-DZ = (0, 1, -1, 2, -4, 5, -5, 6, -6, 7, -7, 8, -2, 3, -3, 4)
-TOKENS = True
+DZ = (0, 1, -1, 2, -2, 3, -3, 4, -6, 7, -7, 8, -4, 5, -5, 6)
 SPLIT = 2
 F32, BF16 = jnp.float32, jnp.bfloat16
 NN = (((1,), (0,)), ((), ()))
@@ -31,10 +30,10 @@
 def kernel(
     nz,
     res_any, mix_gain, pool_w, pool_scale, ffn_gain, ids, wts, gate_any, up_any, down_any,
-    out_any,
+    out,
     res, gate, up, down, ng, rim, aft, pick, code, sel, cols,
-    sent, slots, part, got1, got2, got3, summed, ret, normed, out,
-    lsem, rim_s, rim_r, dsp_s, dsp_r, ret_s, ret_r, own_s, ag_s, ag_r, rs_s, rs_r, og_s, og_r, out_s, tokp, tokm,
+    sent, slots, part, got1, got2, got3, summed, ret, normed,
+    lsem, rim_s, rim_r, dsp_s, dsp_r, ret_s, ret_r, own_s, ag_s, ag_r, rs_s, rs_r, og_s, og_r, tok,
 ):
     tokens, width = res.shape
     group = width // GROUPS
@@ -48,9 +47,15 @@
     def along(axis, d):
         return {axis: ({"x": x, "y": y}[axis] + d) % 4}
 
+    loads = [
+        pltpu.make_async_copy(s, d, lsem.at[i])
+        for i, (s, d) in enumerate(((res_any, res), (gate_any, gate), (up_any, up), (down_any, down)))
+    ]
+    for copy in loads:
+        copy.start()
+
     barrier = pltpu.get_barrier_semaphore()
-    reach = (0, 1, nz - 1) if TOKENS else range(nz)
-    for r in reach:
+    for r in (0, 1, 2, nz - 2, nz - 1):
         for rel in range(2):
             if r or rel:
                 pl.semaphore_signal(
@@ -60,24 +65,12 @@
         for d in (1, 2, 3):
             pl.semaphore_signal(barrier, 1, device_id=along(axis, d), device_id_type=MESH)
 
-    loads = [
-        pltpu.make_async_copy(s, d, lsem.at[i])
-        for i, (s, d) in enumerate(((res_any, res), (gate_any, gate), (up_any, up), (down_any, down)))
-    ]
-    for copy in loads:
-        copy.start()
-
-    def pass_on(h):
-        if not TOKENS:
-            return
-        if h > 1:
-            pl.semaphore_wait(tokp.at[h], 1)
-            if h < nz // 2:
-                pl.semaphore_wait(tokm.at[h], 1)
-        if h < nz // 2:
-            pl.semaphore_signal(tokp.at[h + 1], 1, device_id={"z": (z + 1) % nz}, device_id_type=MESH)
-        if h < nz // 2 - 1:
-            pl.semaphore_signal(tokm.at[h + 1], 1, device_id={"z": (z + nz - 1) % nz}, device_id_type=MESH)
+    def tell(r):
+        for d in (r, nz - r):
+            pl.semaphore_signal(tok.at[r // 4], 1, device_id={"z": (z + d) % nz}, device_id_type=MESH)
+
+    def told(r):
+        pl.semaphore_wait(tok.at[r // 4], 2)
 
     window = lax.shift_left(jnp.int32(1), y + 1)
     first = pl.multiple_of(y * group, group)
@@ -105,18 +98,17 @@
 
     loads[0].wait()
     norm_rows(tokens - 32, 32)
-    pl.semaphore_wait(barrier, 11 if TOKENS else nz * 2 + 5)
+    pl.semaphore_wait(barrier, 15)
     nxt = {"z": (z + c) % nz, "c": (c + 1) % 2}
     rim_copy = pltpu.make_async_remote_copy(
         src_ref=ng.at[pl.ds(tokens - SPAN, SPAN)], dst_ref=rim, send_sem=rim_s, recv_sem=rim_r,
         device_id=nxt, device_id_type=MESH,
     )
     rim_copy.start()
-    pass_on(1)
+    tell(2)
 
     for b in range(tokens // 32 - 1):
         norm_rows(b * 32, 32)
-    pass_on(2)
 
     mine = pl.multiple_of((y * 4 + x) * 128, 128)
     start = (z * 2 + c) * tokens
@@ -132,7 +124,6 @@
     mixed_rows(mm(band, ng[...]), tokens)
     for e in range(experts):
         pick[e * blk : (e + 1) * blk, :] = jnp.where(code[e : e + 1, :] == place, 1.0, 0.0).astype(BF16)
-    pass_on(3)
 
     rim_copy.wait_recv()
     ri = lax.broadcasted_iota(jnp.int32, (SPAN, SPAN), 0)
@@ -142,11 +133,7 @@
     mixed_rows(mm(bend, ng[0:SPAN, :]) + mm(over.astype(BF16), rim[...]), SPAN)
 
     sent[...] = mm(pick[...], aft[...]).astype(BF16)
-    known = 3
-    for r, dz in enumerate(DZ):
-        while known < abs(dz):
-            known += 1
-            pass_on(known)
+    def dispatch(r, dz):
         for rel in range(2):
             zd, cd = (z + (nz - dz) % nz) % nz, (c + rel) % 2
             src = sent.at[pl.ds(pl.multiple_of((zd * 2 + cd) * blk, blk), blk)]
@@ -160,9 +147,19 @@
             else:
                 pltpu.make_async_copy(src, dst, own_s.at[0]).start()
 
-    lane = lax.broadcasted_iota(jnp.int32, (tokens, experts * blk), 1).astype(F32)
-    for k in range(2):
-        sel[k * tokens : (k + 1) * tokens, :] = jnp.where(cols[:, k : k + 1] == lane, 1.0, 0.0).astype(BF16)
+    for r in range(4):
+        dispatch(r, DZ[r])
+    told(2)
+    tell(4)
+    later = sorted(range(4, nz), key=lambda r: abs(DZ[r]))
+    for r in later:
+        if abs(DZ[r]) <= 4:
+            dispatch(r, DZ[r])
+
+    def fill_selection():
+        lane = lax.broadcasted_iota(jnp.int32, (tokens, experts * blk), 1).astype(F32)
+        for k in range(2):
+            sel[k * tokens : (k + 1) * tokens, :] = jnp.where(cols[:, k : k + 1] == lane, 1.0, 0.0).astype(BF16)
 
     def landed(ref, sem):
         pltpu.make_async_copy(ref, ref, sem).wait()
@@ -196,53 +193,42 @@
         def a1(k):
             for d in (1, 3, 2):
                 for h, ax, _ in HALVES:
-                    push(one(h, 0, k, 0, hl), one(h, 0, k, 0, hl), ss.at[k, 0, h, d - 1], rs.at[k, 0, h, d - 1], along(ax, d))
+                    push(one(h, 0, k, 0, hl), one(h, 0, k, 0, hl), ss.at[k], rs.at[k, h, 0], along(ax, d))
 
         def a2(k):
             for h, _, ax in HALVES:
-                for d in (1, 3, 2):
-                    landed(one(h, 4 - d, k, 0, hl), rs.at[k, 0, h, d - 1])
+                landed(buf.at[0, pl.ds(0, 3), rows(k, h, 0, hl)], rs.at[k, h, 0])
                 for i, d in DIRS:
                     ref = line(h, 0, k, 0, hl)
-                    push(ref, ref, ss.at[k, 1, h, i], rs.at[k, 1, h, i], along(ax, d))
+                    push(ref, ref, ss.at[k], rs.at[k, h, 1 + i], along(ax, d))
 
         def a3(k):
             for h, _, ax in HALVES:
                 for i, d, off, n in pieces(hl):
-                    landed(line(h, 4 - d, k, 0, hl), rs.at[k, 1, h, i])
+                    landed(line(h, 4 - d, k, 0, hl), rs.at[k, h, 1 + i])
                     ref = line(h, 4 - d, k, off, n)
-                    push(ref, ref, ss.at[k, 2, h, i], rs.at[k, 2, h, i], along(ax, d))
+                    push(ref, ref, ss.at[k], rs.at[k, h, 3], along(ax, d))
 
         def a4(k):
             for h, _, _ in HALVES:
-                for i, d, off, n in pieces(hl):
-                    landed(line(h, 2, k, off, n), rs.at[k, 2, h, i])
+                landed(line(h, 2, k, 0, hl), rs.at[k, h, 3])
 
         def drain(k):
-            for h in (0, 1):
-                for d in (1, 2, 3):
-                    landed(one(h, 0, k, 0, hl), ss.at[k, 0, h, d - 1])
-                for i, _, off, n in pieces(hl):
-                    landed(line(h, 0, k, 0, hl), ss.at[k, 1, h, i])
-                    landed(line(h, 0, k, 0, n), ss.at[k, 2, h, i])
+            landed(buf.at[:, :, pl.ds(0, hl * 15 // 8)], ss.at[k])
 
         return a1, a2, a3, a4, drain
 
     def base_of(k):
-        return pl.multiple_of(k * chunk, chunk)
+        return k * chunk if isinstance(k, int) else pl.multiple_of(k * chunk, chunk)
 
     a1, a2, a3, a4, ag_drain = gather_stages(slots, base_of, half, ag_s, ag_r)
 
     def s0(k):
-        @pl.when(k == 0)
-        def _():
+        if isinstance(k, int):
             landed(slots.at[y, x, pl.ds(0, blk)], own_s.at[0])
             landed(slots.at[y, x, pl.ds(blk, chunk - blk)], dsp_r.at[0])
-
-        @pl.when(k > 0)
-        def _():
+        else:
             landed(slots.at[y, x, pl.ds(base_of(k), chunk)], dsp_r.at[k])
-
         a1(k)
 
     def line(h, d, k, off, n):
@@ -293,7 +279,7 @@
             part[t // 4, t % 4 + 1, rows, :] = p[:, 128:]
         for h, ax, _ in SUMS:
             for i, d, off, n in pieces(half):
-                push(line(h, 2, k, off, n), got1.at[k, h, :, pl.ds(off, n)], rs_s.at[k, 0, h, i], rs_r.at[k, 0, h, i], along(ax, d))
+                push(line(h, 2, k, off, n), got1.at[k, h, :, pl.ds(off, n)], rs_s.at[k], rs_r.at[k, h, i], along(ax, d))
 
     def add(ref, *others):
         total = ref[...].astype(F32)
@@ -304,24 +290,22 @@
     def r2(k):
         for h, ax, _ in SUMS:
             for i, d, off, n in pieces(half):
-                landed(got1.at[k, h, :, pl.ds(off, n)], rs_r.at[k, 0, h, i])
+                landed(got1.at[k, h, :, pl.ds(off, n)], rs_r.at[k, h, i])
                 add(line(h, d, k, off, n), got1.at[k, h, :, pl.ds(off, n)])
-                push(line(h, d, k, 0, half), got2.at[k, h, i], rs_s.at[k, 1, h, i], rs_r.at[k, 1, h, i], along(ax, d))
+                push(line(h, d, k, 0, half), got2.at[k, h, i], rs_s.at[k], rs_r.at[k, h, 2], along(ax, d))
 
     def r3(k):
         for h, _, ax in SUMS:
-            for i, d in DIRS:
-                landed(got2.at[k, h, i], rs_r.at[k, 1, h, i])
+            landed(got2.at[k, h], rs_r.at[k, h, 2])
             add(line(h, 0, k, 0, half), got2.at[k, h, 0], got2.at[k, h, 1])
             for d in (2, 1, 3):
-                push(one(h, d, k, 0, half), got3.at[k, h, d - 1], rs_s.at[k, 2, h, d - 1], rs_r.at[k, 2, h, d - 1], along(ax, d))
+                push(one(h, d, k, 0, half), got3.at[k, h, d - 1], rs_s.at[k], rs_r.at[k, h, 3], along(ax, d))
 
     home = pl.ds(pl.multiple_of((z * 2 + c) * blk, blk), blk)
 
     def back(k):
         for h, _, _ in SUMS:
-            for d in (1, 3, 2):
-                landed(got3.at[k, h, d - 1], rs_r.at[k, 2, h, d - 1])
+            landed(got3.at[k, h], rs_r.at[k, h, 3])
             total = one(h, 0, k, 0, half)[...].astype(F32)
             for d in (1, 2, 3):
                 total = total + got3[k, h, d - 1].astype(F32)
@@ -340,12 +324,7 @@
                         pltpu.make_async_copy(src, ret.at[home], own_s.at[1]).start()
 
     def rs_drain(k):
-        for h in (0, 1):
-            for i, _, off, n in pieces(half):
-                landed(got1.at[k, h, :, pl.ds(off, n)], rs_s.at[k, 0, h, i])
-                landed(got2.at[k, h, i], rs_s.at[k, 1, h, i])
-            for d in (1, 2, 3):
-                landed(got3.at[k, h, d - 1], rs_s.at[k, 2, h, d - 1])
+        landed(part.at[:, :, pl.ds(0, chunk * 15 // 16)], rs_s.at[k])
 
     stages = (s0, a2, a3, ffn, r2, r3, back)
 
@@ -359,7 +338,13 @@
 
         return carry
 
-    lax.fori_loop(0, NC + len(stages) - 1, step, 0)
+    s0(0)
+    told(4)
+    for r in later:
+        if abs(DZ[r]) > 4:
+            dispatch(r, DZ[r])
+    fill_selection()
+    lax.fori_loop(1, NC + len(stages) - 1, step, 0)
 
     landed(ret.at[pl.ds(0, blk)], own_s.at[1])
     landed(ret.at[pl.ds(blk, (experts - 1) * blk)], ret_r)
@@ -372,13 +357,6 @@
         for s, stage in enumerate(over_out):
             if 0 <= tau - s < NO:
                 stage(tau - s)
-    puts = [
-        pltpu.make_async_copy(out.at[t // 4, t % 4], out_any.at[:, pl.ds(t * 128, 128)], out_s.at[t])
-        for t in range(16)
-    ]
-    for copy in puts:
-        copy.start()
-
     rim_copy.wait_send()
     landed(sent.at[pl.ds(0, (experts - 1) * blk)], dsp_s)
     landed(summed.at[pl.ds(0, (experts - 1) * blk)], ret_s)
@@ -391,7 +369,16 @@
     lax.fori_loop(0, NC, drains, 0)
     for k in range(NO):
         og_drain(k)
-    for copy in puts:
+
+
+def lay_out(src, dst, sem):
+    copies = [
+        pltpu.make_async_copy(src.at[t // 4, t % 4], dst.at[:, pl.ds(t * 128, 128)], sem.at[t])
+        for t in range(16)
+    ]
+    for copy in copies:
+        copy.start()
+    for copy in copies:
         copy.wait()
 
 
@@ -408,9 +395,9 @@
     out = pl.pallas_call(
         functools.partial(kernel, nz),
         name="layer",
-        out_shape=jax.ShapeDtypeStruct((tokens, width), BF16),
+        out_shape=pltpu.VMEM((4, 4, tokens, 128), BF16),
         in_specs=[hbm, vmem, vmem, vmem, vmem, vmem, vmem, hbm, hbm, hbm],
-        out_specs=hbm,
+        out_specs=vmem,
         scratch_shapes=[
             V((tokens, width), BF16),
             V((ff, width), BF16),
@@ -432,21 +419,28 @@
             V((total, 128), BF16),
             V((total, 128), BF16),
             V((chunk, width), BF16),
-            V((4, 4, tokens, 128), BF16),
             dma((4,)),
             dma, dma, dma, dma((NC,)), dma, dma, dma((2,)),
-            dma((NC, 3, 2, 3)), dma((NC, 3, 2, 3)), dma((NC, 3, 2, 3)), dma((NC, 3, 2, 3)),
-            dma((NO, 3, 2, 3)), dma((NO, 3, 2, 3)), dma((16,)),
-            pltpu.SemaphoreType.REGULAR((9,)), pltpu.SemaphoreType.REGULAR((9,)),
+            dma((NC,)), dma((NC, 2, 4)), dma((NC,)), dma((NC, 2, 4)),
+            dma((NO,)), dma((NO, 2, 4)),
+            pltpu.SemaphoreType.REGULAR((2,)),
         ],
         compiler_params=pltpu.CompilerParams(
-            collective_id=0, has_side_effects=True, vmem_limit_bytes=60 * 1024 * 1024
+            collective_id=0, has_side_effects=True, vmem_limit_bytes=58 * 1024 * 1024
         ),
     )(
         res, mix_gain.reshape(1, -1), pool_w, pool_scale.reshape(1, -1), ffn_gain.reshape(1, -1),
         ids.T, wts.T, gate[0].T, up[0].T, down[0],
     )
-    return out
+    return pl.pallas_call(
+        lay_out,
+        name="lay_out",
+        out_shape=jax.ShapeDtypeStruct((tokens, width), BF16),
+        in_specs=[vmem],
+        out_specs=hbm,
+        scratch_shapes=[dma((16,))],
+        compiler_params=pltpu.CompilerParams(vmem_limit_bytes=4 * 1024 * 1024),
+    )(out)
 
 
 def solution(mesh):

time: 105 us -> 98.2 us (0.935)
  Pallas kernels: 103 us -> 98.1 us
  local copies, waits for them, and re-layouts: 2.3 us -> 0 us
    pallas_call x1 -> x2, Pallas kernels: 103 us -> 98.1 us  [the longest x1 97 us: shards(): pl.pallas_call(functools.partial(kernel, nz), name='layer', out_shape=plt...]
    unnamed x1 -> x0, local copies, waits for them, and re-layouts: 2.3 us -> none
where the time goes in v3:
time: 98.2 us; the launch traced here: 98.1 us
  Pallas kernels  98.1 us (100%)
    pallas_call x1, Pallas kernels, shards(): pl.pallas_call(functools.partial(kernel, nz), name='layer', out_shape=plt...  97 us

profile of v3, /device:TPU:32, one launch (start us, length us, event | category | flops | bytes accessed | tf_op | source)
XLA Modules:
  0.0 98.1 jit_solution(3049027847644537210)
XLA Ops:
  0.0 97.0 %layer.1.src = bf16[4,4,256,128]{3,2,1,0:T(8,128)(2,1)S(1)} custom-call(bf16[256,2048]{1,0:T(8,128)(2,1)} %res_any.1, f32[1,2048]{1,0:T(1,128)} %bitcast.15, bf16[512,128]{1,0:T(8,128)(2,1)} %pool_w.1, f32[1,128]{1,0:T(1,128)} %bitcast.19, f32[1,2048]{1,0:T(1,128)} %bitcast.16, s32[2,256]{1,0:T(2,128)} %bitcast.17, f32[2,256]{1,0:T(2,128)} %bitcast.18, ...), custom_call_target="tpu_custom_call" | custom-call | tf_op jit(solution)/shard_map/layer/pallas_call | solution.py:395
  97.0 1.1 %lay_out.1 = bf16[256,2048]{1,0:T(8,128)(2,1)} custom-call(bf16[4,4,256,128]{3,2,1,0:T(8,128)(2,1)S(1)} %layer.1.src), custom_call_target="tpu_custom_call" | custom-call | tf_op jit(solution)/shard_map/lay_out/pallas_call | solution.py:435

commit v4 on v3

--- a/solution.py
+++ b/solution.py
@@ -29,9 +29,9 @@
 
 def kernel(
     nz,
-    res_any, mix_gain, pool_w, pool_scale, ffn_gain, ids, wts, gate_any, up_any, down_any,
+    res_any, mix_any, pw_any, ps_any, ffn_any, ids_any, wts_any, gate_any, up_any, down_any,
     out,
-    res, gate, up, down, ng, rim, aft, pick, code, sel, cols,
+    mix_gain, pool_w, pool_scale, ffn_gain, ids, wts, res, gate, up, down, ng, rim, aft, pick, code, sel, cols,
     sent, slots, part, got1, got2, got3, summed, ret, normed,
     lsem, rim_s, rim_r, dsp_s, dsp_r, ret_s, ret_r, own_s, ag_s, ag_r, rs_s, rs_r, og_s, og_r, tok,
 ):
@@ -49,9 +49,14 @@
 
     loads = [
         pltpu.make_async_copy(s, d, lsem.at[i])
-        for i, (s, d) in enumerate(((res_any, res), (gate_any, gate), (up_any, up), (down_any, down)))
+        for i, (s, d) in enumerate(
+            (
+                (ids_any, ids), (wts_any, wts), (res_any, res), (mix_any, mix_gain), (pw_any, pool_w),
+                (ps_any, pool_scale), (ffn_any, ffn_gain), (gate_any, gate), (up_any, up), (down_any, down),
+            )
+        )
     ]
-    for copy in loads:
+    for copy in loads[:6]:
         copy.start()
 
     barrier = pltpu.get_barrier_semaphore()
@@ -74,14 +79,15 @@
 
     window = lax.shift_left(jnp.int32(1), y + 1)
     first = pl.multiple_of(y * group, group)
-    gain = mix_gain[:, pl.ds(first, group)]
-
     def norm_rows(at, n):
         rows = pl.ds(at, n)
+        gain = mix_gain[:, pl.ds(first, group)]
         v = res[rows, :].astype(F32)
         inv = lax.rsqrt(jnp.sum(v * v, axis=1, keepdims=True) / width + EPS)
         ng[rows, :] = (res[rows, pl.ds(first, group)].astype(F32) * inv * gain).astype(BF16)
 
+    for copy in loads[:2]:
+        copy.wait()
     eid = lax.broadcasted_iota(jnp.int32, (experts, tokens), 0)
     m0, m1 = ids[0:1, :] == eid, ids[1:2, :] == eid
     ti = lax.broadcasted_iota(jnp.int32, (tokens, tokens), 0)
@@ -96,7 +102,10 @@
     cols[...] = jnp.transpose(tall)
     place = lax.broadcasted_iota(jnp.int32, (blk, tokens), 0).astype(F32)
 
-    loads[0].wait()
+    for copy in loads[2:6]:
+        copy.wait()
+    for copy in loads[6:]:
+        copy.start()
     norm_rows(tokens - 32, 32)
     pl.semaphore_wait(barrier, 15)
     nxt = {"z": (z + c) % nz, "c": (c + 1) % 2}
@@ -176,7 +185,7 @@
         cut = hl * SPLIT // 4
         return ((0, 1, 0, cut), (1, 3, cut, hl - cut))
 
-    def gather_stages(buf, base_of, hl, ss, rs):
+    def gather_stages(buf, base_of, hl, ss, rs, direct=False):
         def rows(k, h, off, n):
             return pl.ds(base_of(k) + h * hl + off, n)
 
@@ -198,7 +207,7 @@
         def a2(k):
             for h, _, ax in HALVES:
                 landed(buf.at[0, pl.ds(0, 3), rows(k, h, 0, hl)], rs.at[k, h, 0])
-                for i, d in DIRS:
+                for i, d in DIRS + ((2, 2),) * direct:
                     ref = line(h, 0, k, 0, hl)
                     push(ref, ref, ss.at[k], rs.at[k, h, 1 + i], along(ax, d))
 
@@ -216,7 +225,12 @@
         def drain(k):
             landed(buf.at[:, :, pl.ds(0, hl * 15 // 8)], ss.at[k])
 
-        return a1, a2, a3, a4, drain
+        def a34(k):
+            for h in (0, 1):
+                for i, d in DIRS + ((2, 2),):
+                    landed(line(h, 4 - d, k, 0, hl), rs.at[k, h, 1 + i])
+
+        return (a1, a2, a34, drain) if direct else (a1, a2, a3, a4, drain)
 
     def base_of(k):
         return k * chunk if isinstance(k, int) else pl.multiple_of(k * chunk, chunk)
@@ -250,7 +264,7 @@
 
         @pl.when(k == 0)
         def _():
-            for copy in loads[1:]:
+            for copy in loads[6:]:
                 copy.wait()
 
         def norm(b, carry):
@@ -314,7 +328,7 @@
 
             @pl.when(k == kk)
             def _(kk=kk):
-                for i in range(per):
+                for i in reversed(range(per)):
                     j = kk * per + i
                     src = summed.at[pl.ds(j * blk, blk)]
                     to = {"z": (z + (DZ[j // 2] + nz) % nz) % nz, "c": (c + j % 2) % 2}
@@ -340,7 +354,7 @@
 
     s0(0)
     told(4)
-    for r in later:
+    for r in sorted(later, key=lambda r: (r // 4, -abs(DZ[r]))):
         if abs(DZ[r]) > 4:
             dispatch(r, DZ[r])
     fill_selection()
@@ -352,8 +366,8 @@
     mix = cols[:, 2:3] * picked[:tokens] + cols[:, 3:4] * picked[tokens:]
     out[y, x, :, :] = (aft[...].astype(F32) + mix).astype(BF16)
     oc = tokens // NO
-    *over_out, og_drain = gather_stages(out, lambda k: k * oc, oc // 2, og_s, og_r)
-    for tau in range(NO + 3):
+    *over_out, og_drain = gather_stages(out, lambda k: k * oc, oc // 2, og_s, og_r, True)
+    for tau in range(NO + len(over_out) - 1):
         for s, stage in enumerate(over_out):
             if 0 <= tau - s < NO:
                 stage(tau - s)
@@ -396,9 +410,15 @@
         functools.partial(kernel, nz),
         name="layer",
         out_shape=pltpu.VMEM((4, 4, tokens, 128), BF16),
-        in_specs=[hbm, vmem, vmem, vmem, vmem, vmem, vmem, hbm, hbm, hbm],
+        in_specs=[hbm] * 10,
         out_specs=vmem,
         scratch_shapes=[
+            V((1, width), F32),
+            V(pool_w.shape, BF16),
+            V((1, 128), F32),
+            V((1, width), F32),
+            V((2, tokens), jnp.int32),
+            V((2, tokens), F32),
             V((tokens, width), BF16),
             V((ff, width), BF16),
             V((ff, width), BF16),
@@ -419,7 +439,7 @@
             V((total, 128), BF16),
             V((total, 128), BF16),
             V((chunk, width), BF16),
-            dma((4,)),
+            dma((10,)),
             dma, dma, dma, dma((NC,)), dma, dma, dma((2,)),
             dma((NC,)), dma((NC, 2, 4)), dma((NC,)), dma((NC, 2, 4)),
             dma((NO,)), dma((NO, 2, 4)),

time: 98.2 us -> 96.1 us (0.979)
  the two profiles are of different devices: /device:TPU:32 before, /device:TPU:1 now
where the time goes in v4:
time: 96.1 us; the launch traced here: 95.9 us
  Pallas kernels  95.9 us (100%)
    pallas_call x1, Pallas kernels, shards(): pl.pallas_call(functools.partial(kernel, nz), name='layer', out_shape=plt...  94.8 us

profile of v4, /device:TPU:1, one launch (start us, length us, event | category | flops | bytes accessed | tf_op | source)
XLA Modules:
  0.0 95.9 jit_solution(319258706760986606)
XLA Ops:
  0.0 94.8 %layer.1.src = bf16[4,4,256,128]{3,2,1,0:T(8,128)(2,1)S(1)} custom-call(bf16[256,2048]{1,0:T(8,128)(2,1)} %res_any.1, f32[1,2048]{1,0:T(1,128)} %bitcast.15, bf16[512,128]{1,0:T(8,128)(2,1)} %pw_any.1, f32[1,128]{1,0:T(1,128)} %bitcast.19, f32[1,2048]{1,0:T(1,128)} %bitcast.16, s32[2,256]{1,0:T(2,128)} %bitcast.17, f32[2,256]{1,0:T(2,128)} %bitcast.18, ...), custom_call_target="tpu_custom_call" | custom-call | tf_op jit(solution)/shard_map/layer/pallas_call | solution.py:409
  94.9 1.1 %lay_out.1 = bf16[256,2048]{1,0:T(8,128)(2,1)} custom-call(bf16[4,4,256,128]{3,2,1,0:T(8,128)(2,1)S(1)} %layer.1.src), custom_call_target="tpu_custom_call" | custom-call | tf_op jit(solution)/shard_map/lay_out/pallas_call | solution.py:455

commit v5 on v4

--- a/solution.py
+++ b/solution.py
@@ -16,7 +16,7 @@
 NC = 4
 ORDER = (2, 1, 0, 3, 4, 5, 6)
 NO = 2
-DZ = (0, 1, -1, 2, -2, 3, -3, 4, -6, 7, -7, 8, -4, 5, -5, 6)
+DZ = (0, 1, -1, 2, -2, 3, -3, 4, -4, 5, -5, 6, -6, 7, -7, 8)
 SPLIT = 2
 F32, BF16 = jnp.float32, jnp.bfloat16
 NN = (((1,), (0,)), ((), ()))
@@ -200,14 +200,14 @@
             return buf.at[:, (x + d) % 4, rows(k, h, off, n)]
 
         def a1(k):
-            for d in (1, 3, 2):
+            for d in (2, 1, 3):
                 for h, ax, _ in HALVES:
                     push(one(h, 0, k, 0, hl), one(h, 0, k, 0, hl), ss.at[k], rs.at[k, h, 0], along(ax, d))
 
         def a2(k):
             for h, _, ax in HALVES:
                 landed(buf.at[0, pl.ds(0, 3), rows(k, h, 0, hl)], rs.at[k, h, 0])
-                for i, d in DIRS + ((2, 2),) * direct:
+                for i, d in ((2, 2),) * direct + DIRS:
                     ref = line(h, 0, k, 0, hl)
                     push(ref, ref, ss.at[k], rs.at[k, h, 1 + i], along(ax, d))
 

time: 96.1 us -> 94 us (0.978)
  the two profiles are of different devices: /device:TPU:1 before, /device:TPU:32 now
where the time goes in v5:
time: 94 us; the launch traced here: 93.9 us
  Pallas kernels  93.8 us (100%)
    pallas_call x1, Pallas kernels, shards(): pl.pallas_call(functools.partial(kernel, nz), name='layer', out_shape=plt...  92.8 us

profile of v5, /device:TPU:32, one launch (start us, length us, event | category | flops | bytes accessed | tf_op | source)
XLA Modules:
  0.0 93.9 jit_solution(10758618112351805551)
XLA Ops:
  0.0 92.8 %layer.1.src = bf16[4,4,256,128]{3,2,1,0:T(8,128)(2,1)S(1)} custom-call(bf16[256,2048]{1,0:T(8,128)(2,1)} %res_any.1, f32[1,2048]{1,0:T(1,128)} %bitcast.15, bf16[512,128]{1,0:T(8,128)(2,1)} %pw_any.1, f32[1,128]{1,0:T(1,128)} %bitcast.19, f32[1,2048]{1,0:T(1,128)} %bitcast.16, s32[2,256]{1,0:T(2,128)} %bitcast.17, f32[2,256]{1,0:T(2,128)} %bitcast.18, ...), custom_call_target="tpu_custom_call" | custom-call | tf_op jit(solution)/shard_map/layer/pallas_call | solution.py:409
  92.8 1.1 %lay_out.1 = bf16[256,2048]{1,0:T(8,128)(2,1)} custom-call(bf16[4,4,256,128]{3,2,1,0:T(8,128)(2,1)S(1)} %layer.1.src), custom_call_target="tpu_custom_call" | custom-call | tf_op jit(solution)/shard_map/lay_out/pallas_call | solution.py:455
